TPU v7x, 32 devices: a whole 2x2x4 slice. The times are simulated.
32 devices in a mesh: ra: 4 (over z), cb: 8 (over y, x, core).
Axes of the slice: x: 2, y: 2, z: 4, core: 2. Of those that a mesh axis runs over, the one named last changes fastest.
Arguments:
- tokens: bfloat16 [2, 128, 3072], P(None, None, 'ra'), may hold values from -70 to 70
- norm_gain: float32 [2, 3072], P(None, 'ra'), may hold values from 0.1 to 1.9
- gate_weight: float32 [2, 3072, 8448], P(None, 'ra', 'cb'), may hold values from -0.109375 to 0.109375
- gate_scale: float32 [2, 8448], P(None, 'cb'), may hold values from 0.5 to 2
- up_weight: float32 [2, 3072, 8448], P(None, 'ra', 'cb'), may hold values from -0.109375 to 0.109375
- up_scale: float32 [2, 8448], P(None, 'cb'), may hold values from 0.5 to 2
- conv_weight: float32 [2, 3, 8448], P(None, None, 'cb'), may hold values from -3.5 to 3.5
- conv_bias: float32 [2, 8448], P(None, 'cb'), may hold values from -3 to 3
- down_weight: float32 [2, 8448, 3072], P(None, 'cb', 'ra'), may hold values from -0.0625 to 0.0625
- down_scale: float32 [2, 3072], P(None, 'ra'), may hold values from 0.5 to 2
Outputs:
- layer_output: bfloat16 [2, 128, 3072], P(None, None, 'ra')
All inputs are finite; a program needn't handle non-finite values.
Results may differ from a plain program's by a relative error of at most 0.014.
Values may be sent and summed in bfloat16 or wider, within the bound.
No kernel may reach another device: no remote copies, remote signals or barrier semaphores. Data moves between devices by JAX's collectives and lax.ppermute only.
A program may use at most 64 MiB of HBM per device.

v0:
```python
import jax
import jax.numpy as jnp
from jax import lax
from jax.sharding import PartitionSpec as P

WIDTH = 3072


eps = 1e-06
residual_keep = 0.5


def causal_mix(gate_seq, conv_taps, conv_shift):
    count = conv_taps.shape[0]
    length = gate_seq.shape[1]
    padded = jnp.pad(gate_seq, ((0, 0), (count - 1, 0), (0, 0)))
    running = jnp.zeros_like(gate_seq) + conv_shift[None, None, :]
    for offset in range(count):
        running = (
            running + conv_taps[offset][None, None, :] * padded[:, offset : offset + length, :]
        )
    return running


def sublayer(current, norm_g, gate_w, gate_s, up_w, up_s, conv_taps, conv_shift, down_w, down_s):
    sequences, length, local_width = current.shape
    row_count = sequences * length
    values = current.astype(jnp.float32).reshape(row_count, local_width)
    squares = jnp.sum(values * values, axis=1)
    scaled = (values * norm_g[None, :]).astype(jnp.bfloat16)
    gate_part = jnp.dot(scaled, gate_w.astype(jnp.bfloat16), preferred_element_type=jnp.float32)
    up_part = jnp.dot(scaled, up_w.astype(jnp.bfloat16), preferred_element_type=jnp.float32)
    gate_sum, up_sum = (
        lax.psum_scatter(gate_part, "ra", scatter_dimension=1, tiled=True),
        lax.psum_scatter(up_part, "ra", scatter_dimension=1, tiled=True),
    )
    square_sum = lax.psum(squares, "ra")
    share_cols = gate_sum.shape[1]
    col_start = lax.axis_index("ra") * share_cols
    col_gate = lax.dynamic_slice_in_dim(gate_s, col_start, share_cols, 0)
    col_up = lax.dynamic_slice_in_dim(up_s, col_start, share_cols, 0)
    used_taps = lax.dynamic_slice_in_dim(conv_taps, col_start, share_cols, 1)
    used_shift = lax.dynamic_slice_in_dim(conv_shift, col_start, share_cols, 0)
    inverse_rms = lax.rsqrt(square_sum / WIDTH + eps)[:, None]
    gate_sum = gate_sum * inverse_rms * col_gate[None, :]
    up_sum = up_sum * inverse_rms * col_up[None, :]
    units = gate_sum.shape[1]
    conv_out = causal_mix(gate_sum.reshape(sequences, length, units), used_taps, used_shift)
    hidden_act = (jax.nn.silu(conv_out) * up_sum.reshape(sequences, length, units)).astype(
        jnp.bfloat16
    )
    hidden_act = hidden_act.reshape(row_count, units)
    hidden_act = lax.all_gather(hidden_act, "ra", axis=1, tiled=True)
    down_part = jnp.dot(hidden_act, down_w.astype(jnp.bfloat16), preferred_element_type=jnp.float32)
    down_sum = lax.psum(down_part, "cb")
    branch = down_sum * down_s[None, :]
    return (
        (residual_keep * values + branch)
        .astype(jnp.bfloat16)
        .reshape(sequences, length, local_width)
    )


def shards(
    tokens,
    norm_gain,
    gate_weight,
    gate_scale,
    up_weight,
    up_scale,
    conv_weight,
    conv_bias,
    down_weight,
    down_scale,
):
    current = tokens
    for layer_index in range(2):
        current = sublayer(
            current,
            norm_gain[layer_index],
            gate_weight[layer_index],
            gate_scale[layer_index],
            up_weight[layer_index],
            up_scale[layer_index],
            conv_weight[layer_index],
            conv_bias[layer_index],
            down_weight[layer_index],
            down_scale[layer_index],
        )
    return current


def solution(mesh):
    in_specs = (
        P(None, None, "ra"),
        P(None, "ra"),
        P(None, "ra", "cb"),
        P(None, "cb"),
        P(None, "ra", "cb"),
        P(None, "cb"),
        P(None, None, "cb"),
        P(None, "cb"),
        P(None, "cb", "ra"),
        P(None, "ra"),
    )
    out_specs = P(None, None, "ra")
    return jax.shard_map(shards, mesh=mesh, in_specs=in_specs, out_specs=out_specs, check_vma=False)
```

profile of v0, /device:TPU:0, one launch (start us, length us, event | category | flops | bytes accessed | tf_op | source)
XLA Modules:
  0.0 304.9 jit_solution(4028201805180705221)
XLA Ops:
  6.5 1.4 slice_reduce_fusion.1
  7.9 3.2 %convert.12 = bf16[2,768,1056]{1,2,0:T(8,128)(2,1)S(1)} convert(f32[2,768,1056]{1,2,0:T(8,128)} %param.12) | non-fusion elementwise | flops 1622016 | bytes 9732096 | tf_op jit(solution)/shard_map/convert.5
  11.1 1.2 convert_multiply_fusion.5
  12.4 0.7 copy-done
  13.1 1.6 fusion.5
  14.7 0.0 reduce-scatter.5.cloned.1.call-update
  14.7 0.0 reduce-scatter.7.cloned.1.call-start
  14.8 3.2 %convert.13 = bf16[2,768,1056]{1,2,0:T(8,128)(2,1)S(1)} convert(f32[2,768,1056]{1,2,0:T(8,128)} %param.14) | non-fusion elementwise | flops 1622016 | bytes 9732096 | tf_op jit(solution)/shard_map/convert.4
  17.9 1.7 copy-done.1
  19.6 1.6 fusion.4
  21.3 0.0 all-reduce.5.cloned.1.call-start
  21.4 3.4 %convert.14 = bf16[2,1056,768]{2,1,0:T(8,128)(2,1)S(1)} convert(f32[2,1056,768]{2,1,0:T(8,128)} %param.18) | non-fusion elementwise | flops 1622016 | bytes 9732096 | tf_op jit(solution)/shard_map/convert.3
  24.8 0.6 fusion.44
  25.4 0.6 fusion.45
  26.0 0.1 fusion.31
  26.1 0.1 fusion.29
  26.2 0.7 fusion.37
  26.9 13.9 %psum.28 = f32[256]{0:T(256)S(1)} all-reduce(f32[256]{0:T(256)S(1)} %bitcast.56), channel_id=1, replica_groups=mesh['ra'=4,'cb'=8] {'ra'}, use_global_device_ids=true, to_apply=%region_2.0 | all-reduce | flops 256 | bytes 2048 | tf_op jit(solution)/shard_map/psum | solution.py:37
  40.8 0.5 add_rsqrt_fusion.1
  41.4 4.3 %reduce-scatter.5.cloned.1.call-done = f32[256,264]{0,1:T(8,128)} async-done(((f32[256,1056]{0,1:T(8,128)}), f32[256,264]{0,1:T(8,128)}) %reduce-scatter.5.cloned.1.call-update) | async-done | bytes 270352 | tf_op jit(solution)/shard_map/reduce_scatter | solution.py:34
  45.7 28.7 %reduce-scatter.7.cloned.1.call-done = f32[256,264]{0,1:T(8,128)} async-done(((f32[256,1056]{0,1:T(8,128)}), f32[256,264]{0,1:T(8,128)}) %reduce-scatter.7.cloned.1.call-update) | async-done | bytes 270352 | tf_op jit(solution)/shard_map/reduce_scatter | solution.py:35
  74.3 1.9 multiply_multiply_fusion.3
  76.2 1.8 reshape.75
  78.0 0.8 reshape.76
  78.8 3.7 %fusion.28 = bf16[2,128,264]{1,0,2:T(2,128)(2,1)S(1)} fusion(f32[2,128,264]{1,0,2:T(2,128)} %reshape.76, f32[2,128,264]{1,0,2:T(2,128)} %reshape.75, f32[264]{0:T(512)} %get-tuple-element.10, f32[264]{0:T(512)S(1)} %get-tuple-element.9, f32[264]{0:T(512)S(1)} %get-tuple-element.8, f32[264]{0:T(512)S(1)} %get-tuple-element.32), kind=kLoop, calls=%fused_computation.49 | loop fusion | flops 811008 | bytes 680064 | tf_op jit(solution)/shard_map/convert_element_type | solution.py:49
  82.6 16.0 %all_gather.6 = bf16[256,1056]{0,1:T(8,128)(2,1)S(1)} all-gather(bf16[256,264]{0,1:T(8,128)(2,1)S(1)} %bitcast.54), channel_id=1, replica_groups=mesh['ra'=4,'cb'=8] {'ra'}, dimensions={1}, use_global_device_ids=true | all-gather | bytes 675840 | tf_op jit(solution)/shard_map/all_gather | solution.py:53
  98.6 1.6 fusion.3
  100.2 0.0 reduce-scatter.11.cloned.1.call-start
  100.3 54.1 %all-reduce.5.cloned.1.call-done = f32[256,768]{1,0:T(8,128)} async-done(((f32[256,768]{1,0:T(8,128)}), f32[256,768]{1,0:T(8,128)}) %all-reduce.5.cloned.1.call-update) | async-done | bytes 786448 | tf_op jit(solution)/shard_map/psum | solution.py:55
  154.4 1.6 fusion.11
  156.0 0.7 copy-done.2
  156.7 3.1 %fusion.1 = f32[256,1056]{0,1:T(8,128)} fusion(bf16[2,768,1056]{1,2,0:T(8,128)(2,1)} %copy-done.1, bf16[256,768]{1,0:T(8,128)(2,1)S(1)} %get-tuple-element.16, f32[768]{0:T(1024)S(1)} %copy-done.9), kind=kOutput, calls=%fused_computation.3 | convolution fusion | flops 415825920 | bytes 3099648 | tf_op jit(solution)/shard_map/dot_general | solution.py:32
  159.8 0.0 reduce-scatter.9.cloned.1.call-start
  159.9 3.2 %fusion.2 = f32[256,1056]{0,1:T(8,128)} fusion(bf16[2,768,1056]{1,2,0:T(8,128)(2,1)} %copy-done, bf16[256,768]{1,0:T(8,128)(2,1)} %copy-done.2, f32[768]{0:T(1024)S(1)} %copy-done.9), kind=kOutput, calls=%fused_computation.5 | convolution fusion | flops 415825920 | bytes 3099648 | tf_op jit(solution)/shard_map/dot_general | solution.py:31
  163.1 0.0 all-reduce.7.cloned.1.call-start
  163.1 1.4 fusion.35
  164.5 0.1 fusion.39
  164.6 12.2 %psum.30 = f32[256]{0:T(256)S(1)} all-reduce(f32[256]{0:T(256)S(1)} %get-tuple-element.15), channel_id=1, replica_groups=mesh['ra'=4,'cb'=8] {'ra'}, use_global_device_ids=true, to_apply=%region_7.8 | all-reduce | flops 256 | bytes 2048 | tf_op jit(solution)/shard_map/psum | solution.py:37
  176.8 10.4 %reduce-scatter.11.cloned.1.call-done = f32[256,264]{0,1:T(8,128)} async-done(((f32[256,1056]{0,1:T(8,128)}), f32[256,264]{0,1:T(8,128)}) %reduce-scatter.11.cloned.1.call-update) | async-done | bytes 270352 | tf_op jit(solution)/shard_map/reduce_scatter | solution.py:35
  187.2 28.5 %reduce-scatter.9.cloned.1.call-done = f32[256,264]{0,1:T(8,128)} async-done(((f32[256,1056]{0,1:T(8,128)}), f32[256,264]{0,1:T(8,128)}) %reduce-scatter.9.cloned.1.call-update) | async-done | bytes 270352 | tf_op jit(solution)/shard_map/reduce_scatter | solution.py:34
  215.8 1.9 multiply_multiply_fusion.1
  217.6 1.8 reshape.78
  219.4 0.8 reshape.79
  220.3 3.7 %fusion.27 = bf16[2,128,264]{1,0,2:T(2,128)(2,1)S(1)} fusion(f32[2,128,264]{1,0,2:T(2,128)} %reshape.79, f32[2,128,264]{1,0,2:T(2,128)} %reshape.78, f32[264]{0:T(512)S(1)} %get-tuple-element.7, f32[264]{0:T(512)S(1)} %get-tuple-element.6, f32[264]{0:T(512)S(1)} %get-tuple-element.5, f32[264]{0:T(512)S(1)} %get-tuple-element.33), kind=kLoop, calls=%fused_computation.48 | loop fusion | flops 811008 | bytes 680064 | tf_op jit(solution)/shard_map/convert_element_type | solution.py:49
  224.0 16.0 %all_gather.7 = bf16[256,1056]{0,1:T(8,128)(2,1)S(1)} all-gather(bf16[256,264]{0,1:T(8,128)(2,1)S(1)} %bitcast.55), channel_id=1, replica_groups=mesh['ra'=4,'cb'=8] {'ra'}, dimensions={1}, use_global_device_ids=true | all-gather | bytes 675840 | tf_op jit(solution)/shard_map/all_gather | solution.py:53
  240.0 1.6 fusion
  241.6 54.3 %all-reduce.7.cloned.1.call-done = f32[256,768]{1,0:T(8,128)} async-done(((f32[256,768]{1,0:T(8,128)}), f32[256,768]{1,0:T(8,128)}) %all-reduce.7.cloned.1.call-update) | async-done | bytes 786448 | tf_op jit(solution)/shard_map/psum | solution.py:55
  295.9 2.1 fusion.9
  (29 shorter events, 0.2 us)
Async XLA Ops:
  6.5 39.1 %reduce-scatter.5.cloned.1.call-start = ((), (), s32[]{:S(2)}) async-start(), calls=%async_computation.4 | async-start | bytes 1351680 | tf_op jit(solution)/shard_map/reduce_scatter | solution.py:34
  7.9 3.2 %copy-start.3 = (bf16[2,128,768]{2,1,0:T(8,128)(2,1)S(1)}, bf16[2,128,768]{2,1,0:T(8,128)(2,1)}, u32[]{:S(2)}) copy-start(bf16[2,128,768]{2,1,0:T(8,128)(2,1)} %param.10) | copy-start | bytes 1179652
  11.1 1.9 copy-start
  14.7 59.6 %reduce-scatter.7.cloned.1.call-start = ((), (), s32[]{:S(2)}) async-start(), calls=%async_computation.5 | async-start | bytes 1351680 | tf_op jit(solution)/shard_map/reduce_scatter | solution.py:35
  17.9 1.7 copy-start.1
  21.3 133.1 %all-reduce.5.cloned.1.call-start = ((), (), s32[]{:S(2)}) async-start(), calls=%async_computation.6 | async-start | bytes 1572864 | tf_op jit(solution)/shard_map/psum | solution.py:55
  21.4 3.4 %copy-start.5 = (f32[2,1056]{1,0:T(2,128)S(1)}, f32[2,1056]{1,0:T(2,128)}, u32[]{:S(2)}) copy-start(f32[2,1056]{1,0:T(2,128)} %param.13) | copy-start | bytes 25348
  21.4 4.0 %copy-start.6 = (f32[2,1056]{1,0:T(2,128)S(1)}, f32[2,1056]{1,0:T(2,128)}, u32[]{:S(2)}) copy-start(f32[2,1056]{1,0:T(2,128)} %param.15) | copy-start | bytes 25348
  21.4 4.7 %copy-start.7 = (f32[2,1056]{1,0:T(2,128)S(1)}, f32[2,1056]{1,0:T(2,128)}, u32[]{:S(2)}) copy-start(f32[2,1056]{1,0:T(2,128)} %param.17) | copy-start | bytes 25348
  21.4 4.8 %copy-start.4 = (f32[2,3,1056]{2,0,1:T(2,128)S(1)}, f32[2,3,1056]{2,0,1:T(2,128)}, u32[]{:S(2)}) copy-start(f32[2,3,1056]{2,0,1:T(2,128)} %param.16) | copy-start | bytes 76036
  98.6 1.7 copy-start.8
  100.2 56.5 %copy-start.9 = (f32[768]{0:T(1024)S(1)}, f32[768]{0:T(1024)}, u32[]{:S(2)}) copy-start(f32[768]{0:T(1024)} %get-tuple-element.13) | copy-start | bytes 9220
  100.2 87.0 %reduce-scatter.11.cloned.1.call-start = ((), (), s32[]{:S(2)}) async-start(), calls=%async_computation.8 | async-start | bytes 1351680 | tf_op jit(solution)/shard_map/reduce_scatter | solution.py:35
  156.0 0.7 copy-start.2
  159.8 56.0 %reduce-scatter.9.cloned.1.call-start = ((), (), s32[]{:S(2)}) async-start(), calls=%async_computation.7 | async-start | bytes 1351680 | tf_op jit(solution)/shard_map/reduce_scatter | solution.py:34
  163.1 132.8 %all-reduce.7.cloned.1.call-start = ((), (), s32[]{:S(2)}) async-start(), calls=%async_computation.9 | async-start | bytes 1572864 | tf_op jit(solution)/shard_map/psum | solution.py:55
Sparse Core Ops, SparseCore 0:
  14.8 30.7 reduce-scatter.4
  48.0 26.3 reduce-scatter.6
  100.4 53.9 all-reduce.4
  159.9 27.2 reduce-scatter.10
  189.4 26.3 reduce-scatter.8
  241.8 54.0 all-reduce.6
where the time goes:
time: 306 us; the launch traced here: 305 us
  waiting for transfers between devices  180 us (59%)
  blocking collectives  58.2 us (19%)
  other arithmetic  26.3 us (9%)
  between operations  13.7 us (4%)
  local copies, waits for them, and re-layouts  13.4 us (4%)
  matrix products  12.7 us (4%)
    psum x2, waiting for transfers between devices, sublayer(): down_sum = lax.psum(down_part, 'cb')  108 us
    reduce_scatter x2, waiting for transfers between devices, sublayer(): lax.psum_scatter(up_part, 'ra', scatter_dimension=1, tiled=True)  39.1 us
    reduce_scatter x2, waiting for transfers between devices, sublayer(): lax.psum_scatter(gate_part, 'ra', scatter_dimension=1, tiled=True)  32.8 us
    all_gather x2, blocking collectives, sublayer(): hidden_act = lax.all_gather(hidden_act, 'ra', axis=1, tiled=True)  32 us
    psum x2, blocking collectives, sublayer(): square_sum = lax.psum(squares, 'ra')  26.1 us
    another operation x3, other arithmetic  9.73 us
    convert_element_type x2, other arithmetic, sublayer(): (jax.nn.silu(conv_out) * up_sum.reshape(sequences, length, units)).astype...  7.42 us
  transfers between devices with their start and end apart: 6, of which 6 were waited for; matrix products, arithmetic and copies ran while one was open for 5% of the time, Pallas kernels for 0%

commit v1 on v0

v1 whole, which is shorter than its diff:
```python
import functools

import jax
import jax.numpy as jnp
from jax import lax
from jax.experimental import pallas as pl
from jax.experimental.pallas import tpu as pltpu
from jax.sharding import PartitionSpec as P

EPS = 1e-06
KEEP = 0.5
EXTRA = 8
F32 = jnp.float32
BF16 = jnp.bfloat16
VMEM = pltpu.VMEM
SMEM = pltpu.SMEM


def factors(count):
    found, prime = [], 2
    while count > 1:
        while count % prime == 0:
            found.append(prime)
            count //= prime
        prime += 1
    return found


def levels(count):
    stride, out = 1, []
    for size in factors(count):
        out.append((size, stride))
        stride *= size
    return out


def shift_pairs(count, size, stride, step):
    pairs = []
    for index in range(count):
        digit = index // stride % size
        pairs.append((index, index + ((digit + step) % size - digit) * stride))
    return pairs


def offsets(plan):
    grid = [()]
    for size, _ in plan:
        grid = [done + (step,) for done in grid for step in range(size)]
    return grid


def member(index, plan, steps):
    out = index
    for (size, stride), step in zip(plan, steps):
        digit = lax.rem(lax.div(index, stride), size)
        out = out + (lax.rem(digit + step, size) - digit) * stride
    return out


def rows_at(start, size, unit):
    begin = start * unit
    if unit % 8 == 0:
        begin = pl.multiple_of(begin, 8)
    return pl.ds(begin, size)


def project_kernel(plan, units, ids, own, other, gain, gate_w, up_w, *rest):
    first = plan[0][0]
    outs, (gate_acc, up_acc, sq_acc, scaled) = rest[:first], rest[first:]
    step = pl.program_id(0)
    half = own.shape[-2]
    side = ids[1]
    squares = []
    for place, source in ((side, own), (1 - side, other)):
        values = source[...].reshape(half, -1).astype(F32)
        scaled[pl.ds(pl.multiple_of(place * half, 8), half), :] = values * gain[...].reshape(1, -1)
        squares.append(values * values)
    ones = jnp.ones((8, squares[0].shape[1]), BF16)
    sq_own, sq_other = [], []
    sums = []
    for sq in squares:
        high = sq.astype(BF16)
        low = (sq - high.astype(F32)).astype(BF16)
        dims = (((1,), (1,)), ((), ()))
        sums.append(
            lax.dot_general(ones, high, dims, preferred_element_type=F32)
            + lax.dot_general(ones, low, dims, preferred_element_type=F32)
        )
    in_order = jnp.where(
        side == 0,
        jnp.concatenate(sums, axis=1),
        jnp.concatenate(sums[::-1], axis=1),
    )
    x = scaled[...].astype(BF16)
    dims = (((0,), (1,)), ((), ()))
    gate = lax.dot_general(gate_w[0].astype(BF16), x, dims, preferred_element_type=F32)
    up = lax.dot_general(up_w[0].astype(BF16), x, dims, preferred_element_type=F32)

    @pl.when(step == 0)
    def _():
        gate_acc[...] = gate
        up_acc[...] = up
        sq_acc[...] = in_order

    @pl.when(step > 0)
    def _():
        gate_acc[...] += gate
        up_acc[...] += up
        sq_acc[...] += in_order

    @pl.when(step == pl.num_programs(0) - 1)
    def _():
        total = sq_acc[...]
        high = total.astype(BF16).astype(F32)
        mid = (total - high).astype(BF16).astype(F32)
        low = total - high - mid
        row = lax.broadcasted_iota(jnp.int32, total.shape, 0)
        packed = jnp.where(row == 0, high, jnp.where(row == 1, mid, jnp.where(row == 2, low, 0.0))).astype(BF16)
        for steps in offsets(plan):
            inner = 0
            for (size, _), at in zip(plan[1:], steps[1:]):
                inner = inner * size + at
            rows = rows_at(member(ids[0], plan, steps), units, units)
            target = outs[steps[0]]
            target[inner, 0:units, :] = gate_acc[rows, :].astype(BF16)
            target[inner, units : 2 * units, :] = up_acc[rows, :].astype(BF16)
            target[inner, 2 * units : 2 * units + EXTRA, :] = packed


def project(plan, units, half, ids, halves, gain, gate_w, up_w, layer):
    count = 1
    for size, _ in plan:
        count *= size
    width, local_units = gate_w.shape[1:]
    block = 256 if width % 256 == 0 else width
    (own, own_at), (other, other_at) = halves
    rows = 2 * half
    full = lambda at: pl.BlockSpec(
        (1,) * (own.ndim - 2) + (half, block),
        lambda k, at=at: at + (k,),
    )
    first = plan[0][0]
    shape = (count // first, 2 * units + EXTRA, rows)
    return pl.pallas_call(
        functools.partial(project_kernel, plan, units),
        grid=(width // block,),
        out_shape=[jax.ShapeDtypeStruct(shape, BF16)] * first,
        in_specs=[
            pl.BlockSpec(memory_space=SMEM),
            full(own_at),
            full(other_at),
            pl.BlockSpec((1, 1, block), lambda k: (layer, 0, k)),
            pl.BlockSpec((1, block, local_units), lambda k: (layer, k, 0)),
            pl.BlockSpec((1, block, local_units), lambda k: (layer, k, 0)),
        ],
        out_specs=[pl.BlockSpec(shape, lambda k: (0, 0, 0))] * first,
        scratch_shapes=[
            VMEM((local_units, rows), F32),
            VMEM((local_units, rows), F32),
            VMEM((8, rows), F32),
            VMEM((rows, block), F32),
        ],
        cost_estimate=pl.CostEstimate(
            flops=4 * rows * width * local_units, bytes_accessed=8 * width * local_units, transcendentals=0
        ),
        name="project",
    )(ids, own, other, gain, gate_w, up_w)


def activate_kernel(units, length, width, taps, ids, params, *rest):
    parts, out = rest[:-1], rest[-1]
    total = sum(part[0].astype(F32) for part in parts[1:]) + parts[0][0].astype(F32)
    square = jnp.sum(total[2 * units :, :], axis=0, keepdims=True)
    inverse = lax.rsqrt(square / width + EPS)
    table = params[0, rows_at(ids[0], units, units), :]
    gate = total[0:units] * inverse * table[:, 0:1]
    up = total[units : 2 * units] * inverse * table[:, 1:2]
    lane = lax.rem(lax.broadcasted_iota(jnp.int32, (1, gate.shape[1]), 1), length)
    conv = table[:, 2:3] + table[:, 3 + taps - 1 : 3 + taps] * gate
    for back in range(1, taps):
        moved = jnp.where(lane >= back, pltpu.roll(gate, back, 1), 0.0)
        conv = conv + table[:, 3 + taps - 1 - back : 3 + taps - back] * moved
    out[...] = (conv / (1.0 + jnp.exp(-conv)) * up).astype(BF16)


def activate(units, length, width, taps, ids, params, parts, layer):
    rows = parts[0].shape[-1]
    block = (1,) + parts[0].shape[1:]
    return pl.pallas_call(
        functools.partial(activate_kernel, units, length, width, taps),
        grid=(1,),
        out_shape=jax.ShapeDtypeStruct((units, rows), BF16),
        in_specs=[
            pl.BlockSpec(memory_space=SMEM),
            pl.BlockSpec((1,) + params.shape[1:], lambda k: (layer, 0, 0)),
        ]
        + [pl.BlockSpec(block, lambda k: (0, 0, 0))] * len(parts),
        out_specs=pl.BlockSpec((units, rows), lambda k: (0, 0)),
        cost_estimate=pl.CostEstimate(
            flops=40 * units * rows, bytes_accessed=10 * units * rows, transcendentals=units * rows
        ),
        name="activate",
    )(ids, params, *parts)


def down_kernel(plan, units, ids, down_w, *rest):
    chunks, (keep, send, hidden, result) = rest[:-4], rest[-4:]
    for steps, chunk in zip(offsets(plan), chunks):
        hidden[rows_at(member(ids[0], plan, steps), units, units), :] = chunk[...].astype(F32)
    result[...] = lax.dot_general(
        hidden[...].astype(BF16),
        down_w[0].astype(BF16),
        (((0,), (0,)), ((), ())),
        preferred_element_type=F32,
    )
    half = keep.shape[0]
    keep[...] = result[pl.ds(pl.multiple_of(ids[1] * half, 8), half), :].astype(BF16)
    send[...] = result[pl.ds(pl.multiple_of((1 - ids[1]) * half, 8), half), :].astype(BF16)


def down(plan, units, ids, down_w, chunks, layer):
    local_units, width = down_w.shape[1:]
    rows = chunks[0].shape[-1]
    half = jax.ShapeDtypeStruct((rows // 2, width), BF16)
    return pl.pallas_call(
        functools.partial(down_kernel, plan, units),
        grid=(1,),
        out_shape=[half, half],
        in_specs=[
            pl.BlockSpec(memory_space=SMEM),
            pl.BlockSpec((1, local_units, width), lambda k: (layer, 0, 0)),
        ]
        + [pl.BlockSpec((units, rows), lambda k: (0, 0))] * len(chunks),
        out_specs=[pl.BlockSpec((rows // 2, width), lambda k: (0, 0))] * 2,
        scratch_shapes=[VMEM((local_units, rows), F32), VMEM((rows, width), F32)],
        cost_estimate=pl.CostEstimate(
            flops=2 * rows * width * local_units, bytes_accessed=4 * width * local_units, transcendentals=0
        ),
        name="down",
    )(ids, down_w, *chunks)


def make_shards(mesh, groups):
    ra, cb = mesh.shape["ra"], mesh.shape["cb"]
    ra_plan = levels(ra)
    cb_plan = levels(cb)
    inner = cb_plan[0]

    def send_ra(x, level, step):
        return lax.ppermute(x, "ra", shift_pairs(ra, *level, step))

    def send_cb(x, level, step=1):
        return lax.ppermute(x, "cb", shift_pairs(cb, *level, step))

    def scatter_sum(parts):
        kept, arrived = parts[0], [send_ra(parts[k], ra_plan[0], k) for k in range(1, ra_plan[0][0])]
        mine = [kept] + arrived
        for depth in range(1, len(ra_plan)):
            size, _ = ra_plan[depth]
            per = mine[0].shape[0] // size
            later = []
            for step in range(1, size):
                block = sum(m[step * per : (step + 1) * per].astype(F32) for m in mine).astype(BF16)
                later.append(send_ra(block, ra_plan[depth], step))
            if per > 1:
                head = sum(m[:per].astype(F32) for m in mine)
                mine = [head.astype(BF16)] + later
            else:
                mine = mine + later
        return mine

    def gather(hidden):
        have = [hidden]
        for level in ra_plan[::-1]:
            have = have + [send_ra(x, level, step) for step in range(1, level[0]) for x in have]
        return have

    def sum_cb(keep, send):
        total = keep.astype(F32) + send_cb(send, inner).astype(F32)
        for level in cb_plan[1:]:
            mine = total.astype(BF16)
            total = mine.astype(F32)
            for step in range(1, level[0]):
                total = total + send_cb(mine, level, step).astype(F32)
        return total

    def shards(tokens, norm_gain, gate_w, gate_s, up_w, up_s, conv_w, conv_b, down_w, down_s):
        layers = gate_w.shape[0]
        sequences, length, local_width = tokens.shape
        width = local_width * ra
        units = gate_w.shape[2] // ra
        taps = conv_w.shape[1]
        me, side = lax.axis_index("ra"), lax.rem(lax.axis_index("cb"), 2)
        ids = jnp.stack([me, side]).astype(jnp.int32)
        first_ids = jnp.stack([me, 0 * side]).astype(jnp.int32)
        params = jnp.concatenate([gate_s[:, None], up_s[:, None], conv_b[:, None], conv_w], axis=1)
        params = jnp.transpose(params, (0, 2, 1))
        gain = norm_gain[:, None, :]
        half = length // 2
        own_tokens = lax.dynamic_slice_in_dim(tokens, side * half, half, 1)
        state = [None] * sequences
        own = [own_tokens[s] for s in range(sequences)]
        for layer in range(layers):
            for s in range(sequences):
                if layer == 0:
                    halves, used = ((tokens, (s, 0)), (tokens, (s, 1))), first_ids
                else:
                    halves, used = ((own[s], (0,)), (state[s], (0,))), ids
                parts = project(ra_plan, units, half, used, halves, gain, gate_w, up_w, layer)
                mine = scatter_sum(parts)
                hidden = activate(units, length, width, taps, ids, params, mine, layer)
                chunks = gather(hidden)
                order = gather_order(ra_plan)
                keep, send = down(ra_plan, units, ids, down_w, [chunks[order.index(o)] for o in offsets(ra_plan)], layer)
                total = sum_cb(keep, send) * down_s[layer][None, :]
                own[s] = (KEEP * own[s].astype(F32) + total).astype(BF16)
                state[s] = send_cb(own[s], inner)
        outs = []
        for s in range(sequences):
            low = jnp.where(side == 0, own[s], state[s])
            high = jnp.where(side == 0, state[s], own[s])
            outs.append(jnp.concatenate([low, high], axis=0))
        return jnp.stack(outs)

    return shards


def gather_order(plan):
    have = [(0,) * len(plan)]
    for depth in range(len(plan) - 1, -1, -1):
        size = plan[depth][0]
        have = have + [
            item[:depth] + ((item[depth] - step) % size,) + item[depth + 1 :]
            for step in range(1, size)
            for item in have
        ]
    return have


def solution(mesh):
    in_specs = (
        P(None, None, "ra"),
        P(None, "ra"),
        P(None, "ra", "cb"),
        P(None, "cb"),
        P(None, "ra", "cb"),
        P(None, "cb"),
        P(None, None, "cb"),
        P(None, "cb"),
        P(None, "cb", "ra"),
        P(None, "ra"),
    )
    return jax.shard_map(
        make_shards(mesh, 2), mesh=mesh, in_specs=in_specs, out_specs=P(None, None, "ra"), check_vma=False
    )
```

time: 306 us -> 162 us (0.53)
  waiting for transfers between devices: 180 us -> 47.4 us
  blocking collectives: 58.2 us -> 0 us
  Pallas kernels: 0 us -> 43.4 us
  starting transfers between devices: 0.21 us -> 38.5 us
  other arithmetic: 26.3 us -> 6.54 us
  between operations: 13.7 us -> 0.32 us
  matrix products: 12.7 us -> 0 us
  local copies, waits for them, and re-layouts: 13.4 us -> 25.6 us
    psum x2 -> x0, waiting for transfers between devices: 108 us -> none  [sublayer(): down_sum = lax.psum(down_part, 'cb')]
    reduce_scatter x4 -> x0, waiting for transfers between devices: 71.9 us -> none  [the longest x2 39.1 us: sublayer(): lax.psum_scatter(up_part, 'ra', scatter_dimension=1, tiled=True)]
    ppermute x0 -> x36, waiting for transfers between devices: none -> 47.4 us  [the longest x20 34 us: send_ra(): return lax.ppermute(x, 'ra', shift_pairs(ra, *level, step))]
    pallas_call x0 -> x12, Pallas kernels: none -> 43.4 us  [the longest x4 21.8 us: project(): pl.pallas_call(functools.partial(project_kernel, plan, units), grid=(widt...]
    ppermute x0 -> x36, starting transfers between devices: none -> 38.5 us  [the longest x20 25.5 us: send_ra(): return lax.ppermute(x, 'ra', shift_pairs(ra, *level, step))]
    all_gather x2 -> x0, blocking collectives: 32 us -> none  [sublayer(): hidden_act = lax.all_gather(hidden_act, 'ra', axis=1, tiled=True)]
    psum x2 -> x0, blocking collectives: 26.1 us -> none  [sublayer(): square_sum = lax.psum(squares, 'ra')]
    unnamed x22 -> x78, local copies, waits for them, and re-layouts: 3.22 us -> 22.9 us
  transfers between devices with their start and end apart: 6 -> 36, of which waited for: 6 -> 21; matrix products, arithmetic and copies ran while one was open for 5% -> 4% of each run, Pallas kernels for 0% -> 20%
where the time goes in v1:
time: 162 us
  waiting for transfers between devices  47.4 us (29%)
  Pallas kernels  43.4 us (27%)
  starting transfers between devices  38.5 us (24%)
  local copies, waits for them, and re-layouts  25.6 us (16%)
  other arithmetic  6.54 us (4%)
    ppermute x20, waiting for transfers between devices, send_ra(): return lax.ppermute(x, 'ra', shift_pairs(ra, *level, step))  34 us
    ppermute x20, starting transfers between devices, send_ra(): return lax.ppermute(x, 'ra', shift_pairs(ra, *level, step))  25.5 us
    unnamed x78, local copies, waits for them, and re-layouts  22.9 us
    pallas_call x4, Pallas kernels, project(): pl.pallas_call(functools.partial(project_kernel, plan, units), grid=(widt...  21.8 us
    ppermute x16, waiting for transfers between devices, send_cb(): return lax.ppermute(x, 'cb', shift_pairs(cb, *level, step))  13.5 us
    ppermute x16, starting transfers between devices, send_cb(): return lax.ppermute(x, 'cb', shift_pairs(cb, *level, step))  13 us
    pallas_call x4, Pallas kernels, down(): pl.pallas_call(functools.partial(down_kernel, plan, units), grid=(1,), ou...  12.8 us
    pallas_call x4, Pallas kernels, activate(): pl.pallas_call(functools.partial(activate_kernel, units, length, width, t...  8.8 us
  transfers between devices with their start and end apart: 36, of which 21 were waited for; matrix products, arithmetic and copies ran while one was open for 4% of the time, Pallas kernels for 20%

profile of v1, /device:TPU:0, one launch (start us, length us, event | category | flops | bytes accessed | tf_op | source)
XLA Modules:
  0.0 161.8 jit_solution(1586415289643859304)
XLA Ops:
  0.0 1.3 broadcast_in_dim.15.gain
  1.3 7.6 %copy.33.gate_w = f32[2,768,1056]{2,1,0:T(8,128)} copy(f32[2,768,1056]{1,2,0:T(8,128)} %param.12) | data formatting | bytes 12976128 | tf_op args[2]
  8.8 7.6 %copy.34.up_w = f32[2,768,1056]{2,1,0:T(8,128)} copy(f32[2,768,1056]{1,2,0:T(8,128)} %param.14) | data formatting | bytes 12976128 | tf_op args[4]
  17.1 5.4 %project.4 = (bf16[2,536,128]{2,1,0:T(8,128)(2,1)}, bf16[2,536,128]{2,1,0:T(8,128)(2,1)}) custom-call(s32[2]{0:T(128)} %pad_add_fusion.1.ids, bf16[2,128,768]{2,1,0:T(8,128)(2,1)} %other.3, bf16[2,128,768]{2,1,0:T(8,128)(2,1)} %other.3, f32[2,1,768]{2,1,0:T(1,128)} %broadcast_in_dim.15.gain, f32[2,768,1056]{2,1,0:T(8,128)} %copy.33.gate_w, ...), custom_call_target="tpu_custom_call" | custom-call | flops 415236096 | bytes 6488064 | tf_op jit(solution)/shard_map/project/pallas_call | solution.py:144
  22.6 3.1 %collective-permute-start = (bf16[2,536,128]{2,1,0:T(8,128)(2,1)}, bf16[2,536,128]{2,1,0:T(8,128)(2,1)S(1)}, u32[]{:S(2)}, u32[]{:S(2)}) collective-permute-start(bf16[2,536,128]{2,1,0:T(8,128)(2,1)} %get-tuple-element.22), channel_id=1, source_target_pairs={{0,8},{8,0},{16,24},{24,16},{1,9},{9,1},{17,25},{25,17},{2,10},{10... | collective-permute-start | bytes 823304 | tf_op jit(solution)/shard_map/ppermute | solution.py:250
  25.7 5.5 %project.6 = (bf16[2,536,128]{2,1,0:T(8,128)(2,1)}, bf16[2,536,128]{2,1,0:T(8,128)(2,1)}) custom-call(s32[2]{0:T(128)} %pad_add_fusion.1.ids, bf16[2,128,768]{2,1,0:T(8,128)(2,1)} %other.3, bf16[2,128,768]{2,1,0:T(8,128)(2,1)} %other.3, f32[2,1,768]{2,1,0:T(1,128)} %broadcast_in_dim.15.gain, f32[2,768,1056]{2,1,0:T(8,128)} %copy.33.gate_w, ...), custom_call_target="tpu_custom_call" | custom-call | flops 415236096 | bytes 6488064 | tf_op jit(solution)/shard_map/project/pallas_call | solution.py:144
  32.6 2.8 %collective-permute-start.1 = (bf16[1,536,128]{2,1,0:T(8,128)(2,1)S(1)}, bf16[1,536,128]{2,1,0:T(8,128)(2,1)S(1)}, u32[]{:S(2)}, u32[]{:S(2)}) collective-permute-start(bf16[1,536,128]{2,1,0:T(8,128)(2,1)S(1)} %add_convert_fusion.3), channel_id=1, source_target_pairs={{0,16},{8,24},{16,0},{24,8},{1,17},{9,25},{17,1},{25,9},{2,18},{10... | collective-permute-start | bytes 411656 | tf_op jit(solution)/shard_map/ppermute | solution.py:250
  35.4 7.0 %collective-permute-done.18.rest_1_ = bf16[2,536,128]{2,1,0:T(8,128)(2,1)S(1)} collective-permute-done((bf16[2,536,128]{2,1,0:T(8,128)(2,1)}, bf16[2,536,128]{2,1,0:T(8,128)(2,1)S(1)}, u32[]{:S(2)}, u32[]{:S(2)}) %collective-permute-start.18) | collective-permute-done | bytes 274464 | tf_op jit(solution)/shard_map/ppermute | solution.py:250
  45.2 1.4 copy.32
  47.2 2.2 %activate.4.rest_0_ = bf16[264,128]{1,0:T(8,128)(2,1)} custom-call(s32[2]{0:T(128)} %pad_add_fusion.ids, f32[2,1056,6]{2,1,0:T(8,128)} %bitcast.18, bf16[2,536,128]{2,1,0:T(8,128)(2,1)} %get-tuple-element.21.rest_0_, bf16[2,536,128]{2,1,0:T(8,128)(2,1)} %copy-done.7, bf16[1,536,128]{2,1,0:T(8,128)(2,1)} %copy-done.15), custom_call_target="tpu_custom_call" | custom-call | flops 1351680 | bytes 337920 | tf_op jit(solution)/shard_map/activate/pallas_call | solution.py:189
  49.4 1.9 %collective-permute-start.2 = (bf16[264,128]{1,0:T(8,128)(2,1)}, bf16[264,128]{1,0:T(8,128)(2,1)S(1)}, u32[]{:S(2)}, u32[]{:S(2)}) collective-permute-start(bf16[264,128]{1,0:T(8,128)(2,1)} %activate.4.rest_0_), channel_id=1, source_target_pairs={{0,16},{8,24},{16,0},{24,8},{1,17},{9,25},{17,1},{25,9},{2,18},{10... | collective-permute-start | bytes 202760 | tf_op jit(solution)/shard_map/ppermute | solution.py:250
  51.3 3.5 %collective-permute-done.2.rest_1_ = bf16[264,128]{1,0:T(8,128)(2,1)S(1)} collective-permute-done((bf16[264,128]{1,0:T(8,128)(2,1)}, bf16[264,128]{1,0:T(8,128)(2,1)S(1)}, u32[]{:S(2)}, u32[]{:S(2)}) %collective-permute-start.2) | collective-permute-done | bytes 67616 | tf_op jit(solution)/shard_map/ppermute | solution.py:250
  54.8 1.7 %collective-permute-start.4 = (bf16[264,128]{1,0:T(8,128)(2,1)S(1)}, bf16[264,128]{1,0:T(8,128)(2,1)S(1)}, u32[]{:S(2)}, u32[]{:S(2)}) collective-permute-start(bf16[264,128]{1,0:T(8,128)(2,1)S(1)} %collective-permute-done.2.rest_1_), channel_id=1, source_target_pairs={{0,8},{8,0},{16,24},{24,16},{1,9},{9,1},{17,25},{25,17},{2,10},{10... | collective-permute-start | bytes 202760 | tf_op jit(solution)/shard_map/ppermute | solution.py:250
  57.2 2.2 %activate.6.rest_0_ = bf16[264,128]{1,0:T(8,128)(2,1)} custom-call(s32[2]{0:T(128)} %pad_add_fusion.ids, f32[2,1056,6]{2,1,0:T(8,128)} %bitcast.19, bf16[2,536,128]{2,1,0:T(8,128)(2,1)} %get-tuple-element.29.rest_0_, bf16[2,536,128]{2,1,0:T(8,128)(2,1)} %copy-done.5, bf16[1,536,128]{2,1,0:T(8,128)(2,1)} %copy-done.13), custom_call_target="tpu_custom_call" | custom-call | flops 1351680 | bytes 337920 | tf_op jit(solution)/shard_map/activate/pallas_call | solution.py:189
  60.9 3.2 %down.4 = (bf16[64,768]{1,0:T(8,128)(2,1)}, bf16[64,768]{1,0:T(8,128)(2,1)}) custom-call(s32[2]{0:T(128)} %pad_add_fusion.ids, f32[2,1056,768]{2,1,0:T(8,128)} %down_w.7, bf16[264,128]{1,0:T(8,128)(2,1)} %activate.4.rest_0_, bf16[264,128]{1,0:T(8,128)(2,1)} %copy-done.24, bf16[264,128]{1,0:T(8,128)(2,1)} %copy-done.26, bf16[264,128]{1,0:T(8,128)(2,1)} %copy-done.29), custom_call_target="tpu_custom_call" | custom-call | flops 207618048 | bytes 3244032 | tf_op jit(solution)/shard_map/down/pallas_call | solution.py:225
  64.1 2.1 %collective-permute-start.21 = (bf16[264,128]{1,0:T(8,128)(2,1)S(1)}, bf16[264,128]{1,0:T(8,128)(2,1)S(1)}, u32[]{:S(2)}, u32[]{:S(2)}) collective-permute-start(bf16[264,128]{1,0:T(8,128)(2,1)S(1)} %copy-done.11), channel_id=1, source_target_pairs={{0,8},{8,0},{16,24},{24,16},{1,9},{9,1},{17,25},{25,17},{2,10},{10... | collective-permute-start | bytes 202760 | tf_op jit(solution)/shard_map/ppermute | solution.py:250
  66.3 2.6 %collective-permute-done.21.rest_2_ = bf16[264,128]{1,0:T(8,128)(2,1)S(1)} collective-permute-done((bf16[264,128]{1,0:T(8,128)(2,1)S(1)}, bf16[264,128]{1,0:T(8,128)(2,1)S(1)}, u32[]{:S(2)}, u32[]{:S(2)}) %collective-permute-start.21) | collective-permute-done | bytes 67616 | tf_op jit(solution)/shard_map/ppermute | solution.py:250
  68.9 1.6 collective-permute-done.22.rest_3_
  71.1 3.2 %down.6 = (bf16[64,768]{1,0:T(8,128)(2,1)}, bf16[64,768]{1,0:T(8,128)(2,1)}) custom-call(s32[2]{0:T(128)} %pad_add_fusion.ids, f32[2,1056,768]{2,1,0:T(8,128)} %down_w.7, bf16[264,128]{1,0:T(8,128)(2,1)} %activate.6.rest_0_, bf16[264,128]{1,0:T(8,128)(2,1)} %copy-done.21, bf16[264,128]{1,0:T(8,128)(2,1)} %copy-done.27, bf16[264,128]{1,0:T(8,128)(2,1)} %copy-done.30), custom_call_target="tpu_custom_call" | custom-call | flops 207618048 | bytes 3244032 | tf_op jit(solution)/shard_map/down/pallas_call | solution.py:225
  74.4 1.6 collective-permute-start.6
  76.9 1.5 collective-permute-start.24
  78.4 1.3 collective-permute-done.6
  79.7 1.6 collective-permute-start.7
  81.9 1.6 collective-permute-start.25
  83.5 1.3 collective-permute-done.7
  84.8 1.8 %collective-permute-done.25 = bf16[64,768]{1,0:T(8,128)(2,1)S(1)} collective-permute-done((bf16[64,768]{1,0:T(8,128)(2,1)S(1)}, bf16[64,768]{1,0:T(8,128)(2,1)S(1)}, u32[]{:S(2)}, u32[]{:S(2)}) %collective-permute-start.25) | collective-permute-done | bytes 98336 | tf_op jit(solution)/shard_map/ppermute | solution.py:253
  88.7 5.4 %project.5 = (bf16[2,536,128]{2,1,0:T(8,128)(2,1)}, bf16[2,536,128]{2,1,0:T(8,128)(2,1)}) custom-call(s32[2]{0:T(128)} %pad_add_fusion.ids, bf16[64,768]{1,0:T(8,128)(2,1)} %copy-done.1, bf16[64,768]{1,0:T(8,128)(2,1)} %copy-done.18, f32[2,1,768]{2,1,0:T(1,128)} %broadcast_in_dim.15.gain, f32[2,768,1056]{2,1,0:T(8,128)} %copy.33.gate_w, ...), custom_call_target="tpu_custom_call" | custom-call | flops 415236096 | bytes 6488064 | tf_op jit(solution)/shard_map/project/pallas_call | solution.py:144
  94.2 1.6 %collective-permute-start.9 = (bf16[2,536,128]{2,1,0:T(8,128)(2,1)}, bf16[2,536,128]{2,1,0:T(8,128)(2,1)S(1)}, u32[]{:S(2)}, u32[]{:S(2)}) collective-permute-start(bf16[2,536,128]{2,1,0:T(8,128)(2,1)} %get-tuple-element.26), channel_id=1, source_target_pairs={{0,8},{8,0},{16,24},{24,16},{1,9},{9,1},{17,25},{25,17},{2,10},{10... | collective-permute-start | bytes 823304 | tf_op jit(solution)/shard_map/ppermute | solution.py:250
  95.8 1.3 collective-permute-done.26.other
  97.8 5.4 %project.7 = (bf16[2,536,128]{2,1,0:T(8,128)(2,1)}, bf16[2,536,128]{2,1,0:T(8,128)(2,1)}) custom-call(s32[2]{0:T(128)} %pad_add_fusion.ids, bf16[64,768]{1,0:T(8,128)(2,1)} %copy-done.3, bf16[64,768]{1,0:T(8,128)(2,1)} %copy-done.17, f32[2,1,768]{2,1,0:T(1,128)} %broadcast_in_dim.15.gain, f32[2,768,1056]{2,1,0:T(8,128)} %copy.33.gate_w, ...), custom_call_target="tpu_custom_call" | custom-call | flops 415236096 | bytes 6488064 | tf_op jit(solution)/shard_map/project/pallas_call | solution.py:144
  103.6 2.7 %collective-permute-start.10 = (bf16[1,536,128]{2,1,0:T(8,128)(2,1)S(1)}, bf16[1,536,128]{2,1,0:T(8,128)(2,1)S(1)}, u32[]{:S(2)}, u32[]{:S(2)}) collective-permute-start(bf16[1,536,128]{2,1,0:T(8,128)(2,1)S(1)} %add_convert_fusion.2), channel_id=1, source_target_pairs={{0,16},{8,24},{16,0},{24,8},{1,17},{9,25},{17,1},{25,9},{2,18},{10... | collective-permute-start | bytes 411656 | tf_op jit(solution)/shard_map/ppermute | solution.py:250
  106.3 8.6 %collective-permute-done.27.rest_1_ = bf16[2,536,128]{2,1,0:T(8,128)(2,1)S(1)} collective-permute-done((bf16[2,536,128]{2,1,0:T(8,128)(2,1)}, bf16[2,536,128]{2,1,0:T(8,128)(2,1)S(1)}, u32[]{:S(2)}, u32[]{:S(2)}) %collective-permute-start.27) | collective-permute-done | bytes 274464 | tf_op jit(solution)/shard_map/ppermute | solution.py:250
  117.4 2.2 %activate.5.rest_0_ = bf16[264,128]{1,0:T(8,128)(2,1)} custom-call(s32[2]{0:T(128)} %pad_add_fusion.ids, f32[2,1056,6]{2,1,0:T(8,128)} %bitcast.20, bf16[2,536,128]{2,1,0:T(8,128)(2,1)} %get-tuple-element.25.rest_0_, bf16[2,536,128]{2,1,0:T(8,128)(2,1)} %copy-done.10, bf16[1,536,128]{2,1,0:T(8,128)(2,1)} %copy-done.16), custom_call_target="tpu_custom_call" | custom-call | flops 1351680 | bytes 337920 | tf_op jit(solution)/shard_map/activate/pallas_call | solution.py:189
  119.6 2.3 %collective-permute-start.11 = (bf16[264,128]{1,0:T(8,128)(2,1)}, bf16[264,128]{1,0:T(8,128)(2,1)S(1)}, u32[]{:S(2)}, u32[]{:S(2)}) collective-permute-start(bf16[264,128]{1,0:T(8,128)(2,1)} %activate.5.rest_0_), channel_id=1, source_target_pairs={{0,16},{8,24},{16,0},{24,8},{1,17},{9,25},{17,1},{25,9},{2,18},{10... | collective-permute-start | bytes 202760 | tf_op jit(solution)/shard_map/ppermute | solution.py:250
  122.0 5.5 %collective-permute-done.11.rest_1_ = bf16[264,128]{1,0:T(8,128)(2,1)S(1)} collective-permute-done((bf16[264,128]{1,0:T(8,128)(2,1)}, bf16[264,128]{1,0:T(8,128)(2,1)S(1)}, u32[]{:S(2)}, u32[]{:S(2)}) %collective-permute-start.11) | collective-permute-done | bytes 67616 | tf_op jit(solution)/shard_map/ppermute | solution.py:250
  128.1 2.2 %activate.7.rest_0_ = bf16[264,128]{1,0:T(8,128)(2,1)} custom-call(s32[2]{0:T(128)} %pad_add_fusion.ids, f32[2,1056,6]{2,1,0:T(8,128)} %bitcast.21, bf16[2,536,128]{2,1,0:T(8,128)(2,1)} %get-tuple-element.33.rest_0_, bf16[2,536,128]{2,1,0:T(8,128)(2,1)} %copy-done.8, bf16[1,536,128]{2,1,0:T(8,128)(2,1)} %copy-done.14), custom_call_target="tpu_custom_call" | custom-call | flops 1351680 | bytes 337920 | tf_op jit(solution)/shard_map/activate/pallas_call | solution.py:189
  130.4 2.5 %collective-permute-start.29 = (bf16[264,128]{1,0:T(8,128)(2,1)}, bf16[264,128]{1,0:T(8,128)(2,1)S(1)}, u32[]{:S(2)}, u32[]{:S(2)}) collective-permute-start(bf16[264,128]{1,0:T(8,128)(2,1)} %activate.7.rest_0_), channel_id=1, source_target_pairs={{0,16},{8,24},{16,0},{24,8},{1,17},{9,25},{17,1},{25,9},{2,18},{10... | collective-permute-start | bytes 202760 | tf_op jit(solution)/shard_map/ppermute | solution.py:250
  134.1 3.2 %down.5 = (bf16[64,768]{1,0:T(8,128)(2,1)}, bf16[64,768]{1,0:T(8,128)(2,1)}) custom-call(s32[2]{0:T(128)} %pad_add_fusion.ids, f32[2,1056,768]{2,1,0:T(8,128)} %down_w.7, bf16[264,128]{1,0:T(8,128)(2,1)} %activate.5.rest_0_, bf16[264,128]{1,0:T(8,128)(2,1)} %copy-done.23, bf16[264,128]{1,0:T(8,128)(2,1)} %copy-done.25, bf16[264,128]{1,0:T(8,128)(2,1)} %copy-done.28), custom_call_target="tpu_custom_call" | custom-call | flops 207618048 | bytes 3244032 | tf_op jit(solution)/shard_map/down/pallas_call | solution.py:225
  137.4 2.0 %collective-permute-start.31 = (bf16[264,128]{1,0:T(8,128)(2,1)S(1)}, bf16[264,128]{1,0:T(8,128)(2,1)S(1)}, u32[]{:S(2)}, u32[]{:S(2)}) collective-permute-start(bf16[264,128]{1,0:T(8,128)(2,1)S(1)} %collective-permute-done.29.rest_1_), channel_id=1, source_target_pairs={{0,8},{8,0},{16,24},{24,16},{1,9},{9,1},{17,25},{25,17},{2,10},{10... | collective-permute-start | bytes 202760 | tf_op jit(solution)/shard_map/ppermute | solution.py:250
  139.4 3.0 %collective-permute-done.30.rest_2_ = bf16[264,128]{1,0:T(8,128)(2,1)S(1)} collective-permute-done((bf16[264,128]{1,0:T(8,128)(2,1)S(1)}, bf16[264,128]{1,0:T(8,128)(2,1)S(1)}, u32[]{:S(2)}, u32[]{:S(2)}) %collective-permute-start.30) | collective-permute-done | bytes 67616 | tf_op jit(solution)/shard_map/ppermute | solution.py:250
  143.9 3.2 %down.7 = (bf16[64,768]{1,0:T(8,128)(2,1)}, bf16[64,768]{1,0:T(8,128)(2,1)}) custom-call(s32[2]{0:T(128)} %pad_add_fusion.ids, f32[2,1056,768]{2,1,0:T(8,128)} %down_w.7, bf16[264,128]{1,0:T(8,128)(2,1)} %activate.7.rest_0_, bf16[264,128]{1,0:T(8,128)(2,1)} %copy-done.22, bf16[264,128]{1,0:T(8,128)(2,1)} %copy-done.31, bf16[264,128]{1,0:T(8,128)(2,1)} %copy-done.32), custom_call_target="tpu_custom_call" | custom-call | flops 207618048 | bytes 3244032 | tf_op jit(solution)/shard_map/down/pallas_call | solution.py:225
  147.2 1.5 collective-permute-start.15
  149.7 1.5 collective-permute-start.33
  151.1 1.3 collective-permute-done.15
  152.5 1.6 collective-permute-start.16
  154.7 1.6 collective-permute-start.34
  156.3 1.4 collective-permute-done.16
  157.7 1.7 %collective-permute-done.34 = bf16[64,768]{1,0:T(8,128)(2,1)S(1)} collective-permute-done((bf16[64,768]{1,0:T(8,128)(2,1)S(1)}, bf16[64,768]{1,0:T(8,128)(2,1)S(1)}, u32[]{:S(2)}, u32[]{:S(2)}) %collective-permute-start.34) | collective-permute-done | bytes 98336 | tf_op jit(solution)/shard_map/ppermute | solution.py:253
  (139 shorter events, 23.3 us)
Async XLA Ops:
  22.6 9.9 %copy-start.6 = (bf16[2,536,128]{2,1,0:T(8,128)(2,1)S(1)}, bf16[2,536,128]{2,1,0:T(8,128)(2,1)}, u32[]{:S(2)}) copy-start(bf16[2,536,128]{2,1,0:T(8,128)(2,1)} %get-tuple-element.21.rest_0_) | copy-start | bytes 823300
  22.6 9.9 %collective-permute-start = (bf16[2,536,128]{2,1,0:T(8,128)(2,1)}, bf16[2,536,128]{2,1,0:T(8,128)(2,1)S(1)}, u32[]{:S(2)}, u32[]{:S(2)}) collective-permute-start(bf16[2,536,128]{2,1,0:T(8,128)(2,1)} %get-tuple-element.22), channel_id=1, source_target_pairs={{0,8},{8,0},{16,24},{24,16},{1,9},{9,1},{17,25},{25,17},{2,10},{10... | collective-permute-start | bytes 823304 | tf_op jit(solution)/shard_map/ppermute | solution.py:250
  31.2 11.2 %collective-permute-start.18 = (bf16[2,536,128]{2,1,0:T(8,128)(2,1)}, bf16[2,536,128]{2,1,0:T(8,128)(2,1)S(1)}, u32[]{:S(2)}, u32[]{:S(2)}) collective-permute-start(bf16[2,536,128]{2,1,0:T(8,128)(2,1)} %get-tuple-element.30), channel_id=1, source_target_pairs={{0,8},{8,0},{16,24},{24,16},{1,9},{9,1},{17,25},{25,17},{2,10},{10... | collective-permute-start | bytes 823304 | tf_op jit(solution)/shard_map/ppermute | solution.py:250
  32.5 14.1 %copy-start.7 = (bf16[2,536,128]{2,1,0:T(8,128)(2,1)}, bf16[2,536,128]{2,1,0:T(8,128)(2,1)S(1)}, u32[]{:S(2)}) copy-start(bf16[2,536,128]{2,1,0:T(8,128)(2,1)S(1)} %collective-permute-done.rest_1_) | copy-start | bytes 823300
  32.6 14.0 %collective-permute-start.1 = (bf16[1,536,128]{2,1,0:T(8,128)(2,1)S(1)}, bf16[1,536,128]{2,1,0:T(8,128)(2,1)S(1)}, u32[]{:S(2)}, u32[]{:S(2)}) collective-permute-start(bf16[1,536,128]{2,1,0:T(8,128)(2,1)S(1)} %add_convert_fusion.3), channel_id=1, source_target_pairs={{0,16},{8,24},{16,0},{24,8},{1,17},{9,25},{17,1},{25,9},{2,18},{10... | collective-permute-start | bytes 411656 | tf_op jit(solution)/shard_map/ppermute | solution.py:250
  42.4 14.2 %copy-start.5 = (bf16[2,536,128]{2,1,0:T(8,128)(2,1)}, bf16[2,536,128]{2,1,0:T(8,128)(2,1)S(1)}, u32[]{:S(2)}) copy-start(bf16[2,536,128]{2,1,0:T(8,128)(2,1)S(1)} %collective-permute-done.18.rest_1_) | copy-start | bytes 823300
  43.4 13.1 %collective-permute-start.19 = (bf16[1,536,128]{2,1,0:T(8,128)(2,1)S(1)}, bf16[1,536,128]{2,1,0:T(8,128)(2,1)S(1)}, u32[]{:S(2)}, u32[]{:S(2)}) collective-permute-start(bf16[1,536,128]{2,1,0:T(8,128)(2,1)S(1)} %add_convert_fusion.1), channel_id=1, source_target_pairs={{0,16},{8,24},{16,0},{24,8},{1,17},{9,25},{17,1},{25,9},{2,18},{10... | collective-permute-start | bytes 411656 | tf_op jit(solution)/shard_map/ppermute | solution.py:250
  49.4 5.4 %collective-permute-start.2 = (bf16[264,128]{1,0:T(8,128)(2,1)}, bf16[264,128]{1,0:T(8,128)(2,1)S(1)}, u32[]{:S(2)}, u32[]{:S(2)}) collective-permute-start(bf16[264,128]{1,0:T(8,128)(2,1)} %activate.4.rest_0_), channel_id=1, source_target_pairs={{0,16},{8,24},{16,0},{24,8},{1,17},{9,25},{17,1},{25,9},{2,18},{10... | collective-permute-start | bytes 202760 | tf_op jit(solution)/shard_map/ppermute | solution.py:250
  51.3 8.4 %collective-permute-start.3 = (bf16[264,128]{1,0:T(8,128)(2,1)}, bf16[264,128]{1,0:T(8,128)(2,1)S(1)}, u32[]{:S(2)}, u32[]{:S(2)}) collective-permute-start(bf16[264,128]{1,0:T(8,128)(2,1)} %activate.4.rest_0_), channel_id=1, source_target_pairs={{0,8},{8,0},{16,24},{24,16},{1,9},{9,1},{17,25},{25,17},{2,10},{10... | collective-permute-start | bytes 202760 | tf_op jit(solution)/shard_map/ppermute | solution.py:250
  54.8 4.8 %collective-permute-start.4 = (bf16[264,128]{1,0:T(8,128)(2,1)S(1)}, bf16[264,128]{1,0:T(8,128)(2,1)S(1)}, u32[]{:S(2)}, u32[]{:S(2)}) collective-permute-start(bf16[264,128]{1,0:T(8,128)(2,1)S(1)} %collective-permute-done.2.rest_1_), channel_id=1, source_target_pairs={{0,8},{8,0},{16,24},{24,16},{1,9},{9,1},{17,25},{25,17},{2,10},{10... | collective-permute-start | bytes 202760 | tf_op jit(solution)/shard_map/ppermute | solution.py:250
  59.4 24.1 %copy-start.37 = (f32[2,768]{1,0:T(2,128)S(1)}, f32[2,768]{1,0:T(2,128)}, u32[]{:S(2)}) copy-start(f32[2,768]{1,0:T(2,128)} %param.19) | copy-start | bytes 18436
  59.4 27.2 %copy-start = (bf16[2,128,768]{2,1,0:T(8,128)(2,1)S(1)}, bf16[2,128,768]{2,1,0:T(8,128)(2,1)}, u32[]{:S(2)}) copy-start(bf16[2,128,768]{2,1,0:T(8,128)(2,1)} %other.3) | copy-start | bytes 1179652
  59.4 6.8 %collective-permute-start.20 = (bf16[264,128]{1,0:T(8,128)(2,1)}, bf16[264,128]{1,0:T(8,128)(2,1)S(1)}, u32[]{:S(2)}, u32[]{:S(2)}) collective-permute-start(bf16[264,128]{1,0:T(8,128)(2,1)} %activate.6.rest_0_), channel_id=1, source_target_pairs={{0,16},{8,24},{16,0},{24,8},{1,17},{9,25},{17,1},{25,9},{2,18},{10... | collective-permute-start | bytes 202760 | tf_op jit(solution)/shard_map/ppermute | solution.py:250
  64.1 10.2 %copy-start.19 = (bf16[64,768]{1,0:T(8,128)(2,1)S(1)}, bf16[64,768]{1,0:T(8,128)(2,1)}, u32[]{:S(2)}) copy-start(bf16[64,768]{1,0:T(8,128)(2,1)} %get-tuple-element.23) | copy-start | bytes 294916
  64.1 10.2 %collective-permute-start.5 = (bf16[64,768]{1,0:T(8,128)(2,1)}, bf16[64,768]{1,0:T(8,128)(2,1)S(1)}, u32[]{:S(2)}, u32[]{:S(2)}) collective-permute-start(bf16[64,768]{1,0:T(8,128)(2,1)} %get-tuple-element.24), channel_id=1, source_target_pairs={{0,1},{1,0},{2,3},{3,2},{4,5},{5,4},{6,7},{7,6},{8,9},{9,8},{10,11... | collective-permute-start | bytes 294920 | tf_op jit(solution)/shard_map/ppermute | solution.py:253
  64.1 4.8 %collective-permute-start.21 = (bf16[264,128]{1,0:T(8,128)(2,1)S(1)}, bf16[264,128]{1,0:T(8,128)(2,1)S(1)}, u32[]{:S(2)}, u32[]{:S(2)}) collective-permute-start(bf16[264,128]{1,0:T(8,128)(2,1)S(1)} %copy-done.11), channel_id=1, source_target_pairs={{0,8},{8,0},{16,24},{24,16},{1,9},{9,1},{17,25},{25,17},{2,10},{10... | collective-permute-start | bytes 202760 | tf_op jit(solution)/shard_map/ppermute | solution.py:250
  66.2 4.3 %collective-permute-start.22 = (bf16[264,128]{1,0:T(8,128)(2,1)S(1)}, bf16[264,128]{1,0:T(8,128)(2,1)S(1)}, u32[]{:S(2)}, u32[]{:S(2)}) collective-permute-start(bf16[264,128]{1,0:T(8,128)(2,1)S(1)} %collective-permute-done.20.rest_1_), channel_id=1, source_target_pairs={{0,8},{8,0},{16,24},{24,16},{1,9},{9,1},{17,25},{25,17},{2,10},{10... | collective-permute-start | bytes 202760 | tf_op jit(solution)/shard_map/ppermute | solution.py:250
  74.3 1.6 %collective-permute-start.23 = (bf16[64,768]{1,0:T(8,128)(2,1)}, bf16[64,768]{1,0:T(8,128)(2,1)S(1)}, u32[]{:S(2)}, u32[]{:S(2)}) collective-permute-start(bf16[64,768]{1,0:T(8,128)(2,1)} %get-tuple-element.32), channel_id=1, source_target_pairs={{0,1},{1,0},{2,3},{3,2},{4,5},{5,4},{6,7},{7,6},{8,9},{9,8},{10,11... | collective-permute-start | bytes 294920 | tf_op jit(solution)/shard_map/ppermute | solution.py:253
  74.4 5.3 %collective-permute-start.6 = (bf16[64,768]{1,0:T(8,128)(2,1)S(1)}, bf16[64,768]{1,0:T(8,128)(2,1)S(1)}, u32[]{:S(2)}, u32[]{:S(2)}) collective-permute-start(bf16[64,768]{1,0:T(8,128)(2,1)S(1)} %add_convert_fusion.13), channel_id=1, source_target_pairs={{0,2},{1,3},{2,0},{3,1},{4,6},{5,7},{6,4},{7,5},{8,10},{9,11},{10,... | collective-permute-start | bytes 294920 | tf_op jit(solution)/shard_map/ppermute | solution.py:253
  76.9 5.0 %collective-permute-start.24 = (bf16[64,768]{1,0:T(8,128)(2,1)S(1)}, bf16[64,768]{1,0:T(8,128)(2,1)S(1)}, u32[]{:S(2)}, u32[]{:S(2)}) collective-permute-start(bf16[64,768]{1,0:T(8,128)(2,1)S(1)} %add_convert_fusion.8), channel_id=1, source_target_pairs={{0,2},{1,3},{2,0},{3,1},{4,6},{5,7},{6,4},{7,5},{8,10},{9,11},{10,... | collective-permute-start | bytes 294920 | tf_op jit(solution)/shard_map/ppermute | solution.py:253
  79.7 5.1 %collective-permute-start.7 = (bf16[64,768]{1,0:T(8,128)(2,1)S(1)}, bf16[64,768]{1,0:T(8,128)(2,1)S(1)}, u32[]{:S(2)}, u32[]{:S(2)}) collective-permute-start(bf16[64,768]{1,0:T(8,128)(2,1)S(1)} %add_convert_fusion.12), channel_id=1, source_target_pairs={{0,4},{1,5},{2,6},{3,7},{4,0},{5,1},{6,2},{7,3},{8,12},{9,13},{10,... | collective-permute-start | bytes 294920 | tf_op jit(solution)/shard_map/ppermute | solution.py:253
  81.9 4.7 %collective-permute-start.25 = (bf16[64,768]{1,0:T(8,128)(2,1)S(1)}, bf16[64,768]{1,0:T(8,128)(2,1)S(1)}, u32[]{:S(2)}, u32[]{:S(2)}) collective-permute-start(bf16[64,768]{1,0:T(8,128)(2,1)S(1)} %add_convert_fusion.7), channel_id=1, source_target_pairs={{0,4},{1,5},{2,6},{3,7},{4,0},{5,1},{6,2},{7,3},{8,12},{9,13},{10,... | collective-permute-start | bytes 294920 | tf_op jit(solution)/shard_map/ppermute | solution.py:253
  86.7 9.1 %copy-start.3 = (bf16[64,768]{1,0:T(8,128)(2,1)}, bf16[64,768]{1,0:T(8,128)(2,1)S(1)}, u32[]{:S(2)}) copy-start(bf16[64,768]{1,0:T(8,128)(2,1)S(1)} %get-tuple-element.40.own) | copy-start | bytes 294916
  86.7 1.4 collective-permute-start.8
  94.2 9.4 %collective-permute-start.9 = (bf16[2,536,128]{2,1,0:T(8,128)(2,1)}, bf16[2,536,128]{2,1,0:T(8,128)(2,1)S(1)}, u32[]{:S(2)}, u32[]{:S(2)}) collective-permute-start(bf16[2,536,128]{2,1,0:T(8,128)(2,1)} %get-tuple-element.26), channel_id=1, source_target_pairs={{0,8},{8,0},{16,24},{24,16},{1,9},{9,1},{17,25},{25,17},{2,10},{10... | collective-permute-start | bytes 823304 | tf_op jit(solution)/shard_map/ppermute | solution.py:250
  95.8 1.3 collective-permute-start.26
  103.2 11.8 %collective-permute-start.27 = (bf16[2,536,128]{2,1,0:T(8,128)(2,1)}, bf16[2,536,128]{2,1,0:T(8,128)(2,1)S(1)}, u32[]{:S(2)}, u32[]{:S(2)}) collective-permute-start(bf16[2,536,128]{2,1,0:T(8,128)(2,1)} %get-tuple-element.34), channel_id=1, source_target_pairs={{0,8},{8,0},{16,24},{24,16},{1,9},{9,1},{17,25},{25,17},{2,10},{10... | collective-permute-start | bytes 823304 | tf_op jit(solution)/shard_map/ppermute | solution.py:250
  103.6 13.1 %copy-start.10 = (bf16[2,536,128]{2,1,0:T(8,128)(2,1)}, bf16[2,536,128]{2,1,0:T(8,128)(2,1)S(1)}, u32[]{:S(2)}) copy-start(bf16[2,536,128]{2,1,0:T(8,128)(2,1)S(1)} %collective-permute-done.9.rest_1_) | copy-start | bytes 823300
  103.6 13.1 %collective-permute-start.10 = (bf16[1,536,128]{2,1,0:T(8,128)(2,1)S(1)}, bf16[1,536,128]{2,1,0:T(8,128)(2,1)S(1)}, u32[]{:S(2)}, u32[]{:S(2)}) collective-permute-start(bf16[1,536,128]{2,1,0:T(8,128)(2,1)S(1)} %add_convert_fusion.2), channel_id=1, source_target_pairs={{0,16},{8,24},{16,0},{24,8},{1,17},{9,25},{17,1},{25,9},{2,18},{10... | collective-permute-start | bytes 411656 | tf_op jit(solution)/shard_map/ppermute | solution.py:250
  115.0 12.5 %copy-start.8 = (bf16[2,536,128]{2,1,0:T(8,128)(2,1)}, bf16[2,536,128]{2,1,0:T(8,128)(2,1)S(1)}, u32[]{:S(2)}) copy-start(bf16[2,536,128]{2,1,0:T(8,128)(2,1)S(1)} %collective-permute-done.27.rest_1_) | copy-start | bytes 823300
  116.0 11.4 %collective-permute-start.28 = (bf16[1,536,128]{2,1,0:T(8,128)(2,1)S(1)}, bf16[1,536,128]{2,1,0:T(8,128)(2,1)S(1)}, u32[]{:S(2)}, u32[]{:S(2)}) collective-permute-start(bf16[1,536,128]{2,1,0:T(8,128)(2,1)S(1)} %add_convert_fusion), channel_id=1, source_target_pairs={{0,16},{8,24},{16,0},{24,8},{1,17},{9,25},{17,1},{25,9},{2,18},{10... | collective-permute-start | bytes 411656 | tf_op jit(solution)/shard_map/ppermute | solution.py:250
  119.6 7.9 %collective-permute-start.11 = (bf16[264,128]{1,0:T(8,128)(2,1)}, bf16[264,128]{1,0:T(8,128)(2,1)S(1)}, u32[]{:S(2)}, u32[]{:S(2)}) collective-permute-start(bf16[264,128]{1,0:T(8,128)(2,1)} %activate.5.rest_0_), channel_id=1, source_target_pairs={{0,16},{8,24},{16,0},{24,8},{1,17},{9,25},{17,1},{25,9},{2,18},{10... | collective-permute-start | bytes 202760 | tf_op jit(solution)/shard_map/ppermute | solution.py:250
  121.9 11.0 %collective-permute-start.12 = (bf16[264,128]{1,0:T(8,128)(2,1)}, bf16[264,128]{1,0:T(8,128)(2,1)S(1)}, u32[]{:S(2)}, u32[]{:S(2)}) collective-permute-start(bf16[264,128]{1,0:T(8,128)(2,1)} %activate.5.rest_0_), channel_id=1, source_target_pairs={{0,8},{8,0},{16,24},{24,16},{1,9},{9,1},{17,25},{25,17},{2,10},{10... | collective-permute-start | bytes 202760 | tf_op jit(solution)/shard_map/ppermute | solution.py:250
  127.5 5.4 %collective-permute-start.13 = (bf16[264,128]{1,0:T(8,128)(2,1)S(1)}, bf16[264,128]{1,0:T(8,128)(2,1)S(1)}, u32[]{:S(2)}, u32[]{:S(2)}) collective-permute-start(bf16[264,128]{1,0:T(8,128)(2,1)S(1)} %collective-permute-done.11.rest_1_), channel_id=1, source_target_pairs={{0,8},{8,0},{16,24},{24,16},{1,9},{9,1},{17,25},{25,17},{2,10},{10... | collective-permute-start | bytes 202760 | tf_op jit(solution)/shard_map/ppermute | solution.py:250
  130.4 29.0 %copy-start.2 = (bf16[64,768]{1,0:T(8,128)(2,1)S(1)}, bf16[64,768]{1,0:T(8,128)(2,1)}, u32[]{:S(2)}) copy-start(bf16[64,768]{1,0:T(8,128)(2,1)} %copy-done.1) | copy-start | bytes 294916
  130.4 29.0 %copy-start.4 = (bf16[64,768]{1,0:T(8,128)(2,1)S(1)}, bf16[64,768]{1,0:T(8,128)(2,1)}, u32[]{:S(2)}) copy-start(bf16[64,768]{1,0:T(8,128)(2,1)} %copy-done.3) | copy-start | bytes 294916
  130.4 7.0 %collective-permute-start.29 = (bf16[264,128]{1,0:T(8,128)(2,1)}, bf16[264,128]{1,0:T(8,128)(2,1)S(1)}, u32[]{:S(2)}, u32[]{:S(2)}) collective-permute-start(bf16[264,128]{1,0:T(8,128)(2,1)} %activate.7.rest_0_), channel_id=1, source_target_pairs={{0,16},{8,24},{16,0},{24,8},{1,17},{9,25},{17,1},{25,9},{2,18},{10... | collective-permute-start | bytes 202760 | tf_op jit(solution)/shard_map/ppermute | solution.py:250
  137.3 9.9 %copy-start.20 = (bf16[64,768]{1,0:T(8,128)(2,1)S(1)}, bf16[64,768]{1,0:T(8,128)(2,1)}, u32[]{:S(2)}) copy-start(bf16[64,768]{1,0:T(8,128)(2,1)} %get-tuple-element.27) | copy-start | bytes 294916
  137.3 9.9 %collective-permute-start.14 = (bf16[64,768]{1,0:T(8,128)(2,1)}, bf16[64,768]{1,0:T(8,128)(2,1)S(1)}, u32[]{:S(2)}, u32[]{:S(2)}) collective-permute-start(bf16[64,768]{1,0:T(8,128)(2,1)} %get-tuple-element.28), channel_id=1, source_target_pairs={{0,1},{1,0},{2,3},{3,2},{4,5},{5,4},{6,7},{7,6},{8,9},{9,8},{10,11... | collective-permute-start | bytes 294920 | tf_op jit(solution)/shard_map/ppermute | solution.py:253
  137.3 5.1 %collective-permute-start.30 = (bf16[264,128]{1,0:T(8,128)(2,1)S(1)}, bf16[264,128]{1,0:T(8,128)(2,1)S(1)}, u32[]{:S(2)}, u32[]{:S(2)}) collective-permute-start(bf16[264,128]{1,0:T(8,128)(2,1)S(1)} %copy-done.12), channel_id=1, source_target_pairs={{0,8},{8,0},{16,24},{24,16},{1,9},{9,1},{17,25},{25,17},{2,10},{10... | collective-permute-start | bytes 202760 | tf_op jit(solution)/shard_map/ppermute | solution.py:250
  137.4 5.9 %collective-permute-start.31 = (bf16[264,128]{1,0:T(8,128)(2,1)S(1)}, bf16[264,128]{1,0:T(8,128)(2,1)S(1)}, u32[]{:S(2)}, u32[]{:S(2)}) collective-permute-start(bf16[264,128]{1,0:T(8,128)(2,1)S(1)} %collective-permute-done.29.rest_1_), channel_id=1, source_target_pairs={{0,8},{8,0},{16,24},{24,16},{1,9},{9,1},{17,25},{25,17},{2,10},{10... | collective-permute-start | bytes 202760 | tf_op jit(solution)/shard_map/ppermute | solution.py:250
  147.2 1.6 collective-permute-start.32
  147.2 5.3 %collective-permute-start.15 = (bf16[64,768]{1,0:T(8,128)(2,1)S(1)}, bf16[64,768]{1,0:T(8,128)(2,1)S(1)}, u32[]{:S(2)}, u32[]{:S(2)}) collective-permute-start(bf16[64,768]{1,0:T(8,128)(2,1)S(1)} %add_convert_fusion.11), channel_id=1, source_target_pairs={{0,2},{1,3},{2,0},{3,1},{4,6},{5,7},{6,4},{7,5},{8,10},{9,11},{10,... | collective-permute-start | bytes 294920 | tf_op jit(solution)/shard_map/ppermute | solution.py:253
  149.7 5.0 %collective-permute-start.33 = (bf16[64,768]{1,0:T(8,128)(2,1)S(1)}, bf16[64,768]{1,0:T(8,128)(2,1)S(1)}, u32[]{:S(2)}, u32[]{:S(2)}) collective-permute-start(bf16[64,768]{1,0:T(8,128)(2,1)S(1)} %add_convert_fusion.6), channel_id=1, source_target_pairs={{0,2},{1,3},{2,0},{3,1},{4,6},{5,7},{6,4},{7,5},{8,10},{9,11},{10,... | collective-permute-start | bytes 294920 | tf_op jit(solution)/shard_map/ppermute | solution.py:253
  152.5 5.2 %collective-permute-start.16 = (bf16[64,768]{1,0:T(8,128)(2,1)S(1)}, bf16[64,768]{1,0:T(8,128)(2,1)S(1)}, u32[]{:S(2)}, u32[]{:S(2)}) collective-permute-start(bf16[64,768]{1,0:T(8,128)(2,1)S(1)} %add_convert_fusion.10), channel_id=1, source_target_pairs={{0,4},{1,5},{2,6},{3,7},{4,0},{5,1},{6,2},{7,3},{8,12},{9,13},{10,... | collective-permute-start | bytes 294920 | tf_op jit(solution)/shard_map/ppermute | solution.py:253
  154.7 4.7 %collective-permute-start.34 = (bf16[64,768]{1,0:T(8,128)(2,1)S(1)}, bf16[64,768]{1,0:T(8,128)(2,1)S(1)}, u32[]{:S(2)}, u32[]{:S(2)}) collective-permute-start(bf16[64,768]{1,0:T(8,128)(2,1)S(1)} %add_convert_fusion.5), channel_id=1, source_target_pairs={{0,4},{1,5},{2,6},{3,7},{4,0},{5,1},{6,2},{7,3},{8,12},{9,13},{10,... | collective-permute-start | bytes 294920 | tf_op jit(solution)/shard_map/ppermute | solution.py:253
  159.5 1.4 collective-permute-start.35
  159.6 1.4 collective-permute-start.17
  (26 other events, 86.2 us)

commit v2 on v1

v2 whole, which is shorter than its diff:
```python
import functools

import jax
import jax.numpy as jnp
from jax import lax
from jax.experimental import pallas as pl
from jax.experimental.pallas import tpu as pltpu
from jax.sharding import PartitionSpec as P

EPS = 1e-06
KEEP = 0.5
EXTRA = 8
F32 = jnp.float32
BF16 = jnp.bfloat16
VMEM = pltpu.VMEM
SMEM = pltpu.SMEM


def factors(count):
    found, prime = [], 2
    while count > 1:
        while count % prime == 0:
            found.append(prime)
            count //= prime
        prime += 1
    return found


def levels(count):
    stride, out = 1, []
    for size in factors(count):
        out.append((size, stride))
        stride *= size
    return out


def shift_pairs(count, size, stride, step):
    pairs = []
    for index in range(count):
        digit = index // stride % size
        pairs.append((index, index + ((digit + step) % size - digit) * stride))
    return pairs


def offsets(plan):
    grid = [()]
    for size, _ in plan:
        grid = [done + (step,) for done in grid for step in range(size)]
    return grid


def member(index, plan, steps):
    out = index
    for (size, stride), step in zip(plan, steps):
        digit = lax.rem(lax.div(index, stride), size)
        out = out + (lax.rem(digit + step, size) - digit) * stride
    return out


def rows_at(start, size, unit):
    begin = start * unit
    if unit % 8 == 0:
        begin = pl.multiple_of(begin, 8)
    return pl.ds(begin, size)


def project_kernel(plan, layer, units, half, groups, ids, own, other, gain, gate_w, up_w, *rest):
    first = plan[0][0]
    outs, (scaled, packed) = rest[:-2], rest[-2:]
    step = pl.program_id(0)
    side = ids[1]
    wide = ((1,), (1,)), ((), ())

    @pl.when(step == 0)
    def _():
        for group, (own_at, other_at) in enumerate(groups):
            sums = []
            for place, source, at in ((side, own, own_at), (1 - side, other, other_at)):
                values = source[at].astype(F32)
                rows = pl.ds(pl.multiple_of(place * half, 8), half)
                scaled[group, rows, :] = values * gain[layer : layer + 1, :]
                squares = values * values
                high = squares.astype(BF16)
                low = (squares - high.astype(F32)).astype(BF16)
                ones = jnp.ones((8, values.shape[1]), BF16)
                sums.append(
                    lax.dot_general(ones, high, wide, preferred_element_type=F32)
                    + lax.dot_general(ones, low, wide, preferred_element_type=F32)
                )
            total = jnp.where(
                side == 0,
                jnp.concatenate(sums, axis=1),
                jnp.concatenate(sums[::-1], axis=1),
            )
            high = total.astype(BF16).astype(F32)
            mid = (total - high).astype(BF16).astype(F32)
            low = total - high - mid
            row = lax.broadcasted_iota(jnp.int32, total.shape, 0)
            packed[group] = jnp.where(row == 0, high, jnp.where(row == 1, mid, jnp.where(row == 2, low, 0.0)))

    rows = 2 * half
    x = scaled[...].reshape(len(groups) * rows, -1).astype(BF16)
    gate = lax.dot_general(gate_w[0, 0].astype(BF16), x, wide, preferred_element_type=F32).astype(BF16)
    up = lax.dot_general(up_w[0, 0].astype(BF16), x, wide, preferred_element_type=F32).astype(BF16)
    for place, steps in enumerate(offsets(plan)):
        inner = 0
        for (size, _), at in zip(plan[1:], steps[1:]):
            inner = inner * size + at

        @pl.when(step == place)
        def _():
            for group in range(len(groups)):
                target = outs[group * first + steps[0]]
                lanes = slice(group * rows, (group + 1) * rows)
                target[inner, 0:units, :] = gate[:, lanes]
                target[inner, units : 2 * units, :] = up[:, lanes]
                target[inner, 2 * units : 2 * units + EXTRA, :] = packed[group].astype(BF16)


def chunk_at(plan, place, ids):
    steps = []
    for size, _ in plan[::-1]:
        steps.append(lax.rem(place, size))
        place = lax.div(place, size)
    return member(ids[0], plan, steps[::-1])


def project(plan, half, ids, own, other, groups, gain, gate_w, up_w, layer):
    _, count, units, width = gate_w.shape
    rows = 2 * half
    first = plan[0][0]
    shape = (count // first, 2 * units + EXTRA, rows)
    weight = pl.BlockSpec((1, 1, units, width), lambda j, ids: (layer, chunk_at(plan, j, ids), 0, 0))
    whole = pl.BlockSpec(memory_space=VMEM)
    number = len(groups) * first
    return pl.pallas_call(
        functools.partial(project_kernel, plan, layer, units, half, groups),
        grid_spec=pltpu.PrefetchScalarGridSpec(
            num_scalar_prefetch=1,
            grid=(count,),
            in_specs=[whole, whole, whole, weight, weight],
            out_specs=[pl.BlockSpec(shape, lambda j, ids: (0, 0, 0))] * number,
            scratch_shapes=[VMEM((len(groups), rows, width), F32), VMEM((len(groups), EXTRA, rows), F32)],
        ),
        out_shape=[jax.ShapeDtypeStruct(shape, BF16)] * number,
        compiler_params=pltpu.CompilerParams(vmem_limit_bytes=16 << 20),
        cost_estimate=pl.CostEstimate(
            flops=4 * rows * width * count * units, bytes_accessed=8 * width * count * units, transcendentals=0
        ),
        name="project",
    )(ids, own, other, gain, gate_w, up_w)


def activate_kernel(layer, units, length, width, taps, params, *rest):
    parts, out = rest[:-1], rest[-1]
    total = sum(part[0].astype(F32) for part in parts)
    square = jnp.sum(total[2 * units :, :], axis=0, keepdims=True)
    inverse = lax.rsqrt(square / width + EPS)
    table = params[layer]
    gate = total[0:units] * inverse * table[:, 0:1]
    up = total[units : 2 * units] * inverse * table[:, 1:2]
    lane = lax.rem(lax.broadcasted_iota(jnp.int32, (1, gate.shape[1]), 1), length)
    conv = table[:, 2:3] + table[:, 3 + taps - 1 : 3 + taps] * gate
    for back in range(1, taps):
        moved = jnp.where(lane >= back, pltpu.roll(gate, back, 1), 0.0)
        conv = conv + table[:, 3 + taps - 1 - back : 3 + taps - back] * moved
    out[...] = (conv / (1.0 + jnp.exp(-conv)) * up).astype(BF16)


def activate(units, length, width, taps, params, parts, layer):
    rows = parts[0].shape[-1]
    whole = pl.BlockSpec(memory_space=VMEM)
    return pl.pallas_call(
        functools.partial(activate_kernel, layer, units, length, width, taps),
        out_shape=jax.ShapeDtypeStruct((units, rows), BF16),
        in_specs=[whole] * (1 + len(parts)),
        out_specs=whole,
        compiler_params=pltpu.CompilerParams(vmem_limit_bytes=8 << 20),
        cost_estimate=pl.CostEstimate(
            flops=40 * units * rows, bytes_accessed=10 * units * rows, transcendentals=units * rows
        ),
        name="activate",
    )(params, *parts)


def down_kernel(plan, units, ids, down_w, *rest):
    chunks, (keep, send, hidden, result) = rest[:-4], rest[-4:]
    for steps, chunk in zip(offsets(plan), chunks):
        hidden[rows_at(member(ids[0], plan, steps), units, units), :] = chunk[...].astype(F32)
    result[...] = lax.dot_general(
        hidden[...].astype(BF16),
        down_w[0].astype(BF16),
        (((0,), (0,)), ((), ())),
        preferred_element_type=F32,
    )
    half = keep.shape[0]
    keep[...] = result[pl.ds(pl.multiple_of(ids[1] * half, 8), half), :].astype(BF16)
    send[...] = result[pl.ds(pl.multiple_of((1 - ids[1]) * half, 8), half), :].astype(BF16)


def down(plan, units, ids, down_w, chunks, layer):
    local_units, width = down_w.shape[1:]
    rows = chunks[0].shape[-1]
    half = jax.ShapeDtypeStruct((rows // 2, width), BF16)
    whole = pl.BlockSpec(memory_space=VMEM)
    return pl.pallas_call(
        functools.partial(down_kernel, plan, units),
        grid=(1,),
        out_shape=[half, half],
        in_specs=[
            pl.BlockSpec(memory_space=SMEM),
            pl.BlockSpec((1, local_units, width), lambda k: (layer, 0, 0)),
        ]
        + [whole] * len(chunks),
        out_specs=[whole] * 2,
        scratch_shapes=[VMEM((local_units, rows), F32), VMEM((rows, width), F32)],
        compiler_params=pltpu.CompilerParams(vmem_limit_bytes=16 << 20),
        cost_estimate=pl.CostEstimate(
            flops=2 * rows * width * local_units, bytes_accessed=4 * width * local_units, transcendentals=0
        ),
        name="down",
    )(ids, down_w, *chunks)


def make_shards(mesh, groups):
    ra, cb = mesh.shape["ra"], mesh.shape["cb"]
    ra_plan = levels(ra)
    cb_plan = levels(cb)
    inner = cb_plan[0]

    def send_ra(x, level, step):
        return lax.ppermute(x, "ra", shift_pairs(ra, *level, step))

    def send_cb(x, level, step=1):
        return lax.ppermute(x, "cb", shift_pairs(cb, *level, step))

    def scatter_sum(parts):
        kept, arrived = parts[0], [send_ra(parts[k], ra_plan[0], k) for k in range(1, ra_plan[0][0])]
        mine = [kept] + arrived
        for depth in range(1, len(ra_plan)):
            size, _ = ra_plan[depth]
            per = mine[0].shape[0] // size
            later = []
            for step in range(1, size):
                block = sum(m[step * per : (step + 1) * per].astype(F32) for m in mine).astype(BF16)
                later.append(send_ra(block, ra_plan[depth], step))
            if per > 1:
                head = sum(m[:per].astype(F32) for m in mine)
                mine = [head.astype(BF16)] + later
            else:
                mine = mine + later
        return mine

    def gather(hidden):
        have = [hidden]
        for level in ra_plan[::-1]:
            have = have + [send_ra(x, level, step) for step in range(1, level[0]) for x in have]
        return have

    def sum_cb(keep, send):
        total = keep.astype(F32) + send_cb(send, inner).astype(F32)
        for level in cb_plan[1:]:
            mine = total.astype(BF16)
            total = mine.astype(F32)
            for step in range(1, level[0]):
                total = total + send_cb(mine, level, step).astype(F32)
        return total

    def shards(tokens, norm_gain, gate_w, gate_s, up_w, up_s, conv_w, conv_b, down_w, down_s):
        layers = gate_w.shape[0]
        sequences, length, local_width = tokens.shape
        width = local_width * ra
        units = gate_w.shape[2] // ra
        taps = conv_w.shape[1]
        me, side = lax.axis_index("ra"), lax.rem(lax.axis_index("cb"), 2)
        ids = jnp.stack([me, side]).astype(jnp.int32)
        first_ids = jnp.stack([me, 0 * side]).astype(jnp.int32)
        params = jnp.concatenate([gate_s[:, None], up_s[:, None], conv_b[:, None], conv_w], axis=1)
        params = jnp.transpose(params, (0, 2, 1))
        params = lax.dynamic_slice_in_dim(params, me * units, units, 1)
        half = length // 2
        by_chunk = lambda w: jnp.swapaxes(w, 1, 2).reshape(layers, ra, units, local_width)
        gate_t, up_t = by_chunk(gate_w), by_chunk(up_w)
        order = gather_order(ra_plan)
        own_tokens = lax.dynamic_slice_in_dim(tokens, side * half, half, 1)
        own = [own_tokens[s] for s in range(sequences)]
        other = [None] * sequences
        first = ra_plan[0][0]
        groups = [((s, slice(0, half)), (s, slice(half, 2 * half))) for s in range(sequences)]
        started = project(ra_plan, half, first_ids, tokens, tokens, groups, norm_gain, gate_t, up_t, 0)
        for layer in range(layers):
            for s in range(sequences):
                if layer == 0:
                    parts = started[s * first : (s + 1) * first]
                else:
                    groups = [(slice(None), slice(None))]
                    parts = project(ra_plan, half, ids, own[s], other[s], groups, norm_gain, gate_t, up_t, layer)
                mine = scatter_sum(parts)
                hidden = activate(units, length, width, taps, params, mine, layer)
                chunks = gather(hidden)
                chunks = [chunks[order.index(steps)] for steps in offsets(ra_plan)]
                keep, send = down(ra_plan, units, ids, down_w, chunks, layer)
                total = sum_cb(keep, send) * down_s[layer][None, :]
                own[s] = (KEEP * own[s].astype(F32) + total).astype(BF16)
                other[s] = send_cb(own[s], inner)
        outs = []
        for s in range(sequences):
            low = jnp.where(side == 0, own[s], other[s])
            high = jnp.where(side == 0, other[s], own[s])
            outs.append(jnp.concatenate([low, high], axis=0))
        return jnp.stack(outs)

    return shards


def gather_order(plan):
    have = [(0,) * len(plan)]
    for depth in range(len(plan) - 1, -1, -1):
        size = plan[depth][0]
        have = have + [
            item[:depth] + ((item[depth] - step) % size,) + item[depth + 1 :]
            for step in range(1, size)
            for item in have
        ]
    return have


def solution(mesh):
    in_specs = (
        P(None, None, "ra"),
        P(None, "ra"),
        P(None, "ra", "cb"),
        P(None, "cb"),
        P(None, "ra", "cb"),
        P(None, "cb"),
        P(None, None, "cb"),
        P(None, "cb"),
        P(None, "cb", "ra"),
        P(None, "ra"),
    )
    return jax.shard_map(
        make_shards(mesh, 2), mesh=mesh, in_specs=in_specs, out_specs=P(None, None, "ra"), check_vma=False
    )
```

time: 162 us -> 136 us (0.84)
  Pallas kernels: 43.4 us -> 14 us
  waiting for transfers between devices: 47.4 us -> 61.8 us
  local copies, waits for them, and re-layouts: 25.6 us -> 16.1 us
  other arithmetic: 6.54 us -> 1.68 us
  starting transfers between devices: 38.5 us -> 42 us
    pallas_call x8 -> x7, Pallas kernels: 30.6 us -> 9.69 us  [the longest x3 8.13 us: project(): pl.pallas_call(functools.partial(project_kernel, plan, layer, units, half...]
    ppermute x20, waiting for transfers between devices: 34 us -> 45.6 us  [send_ra(): return lax.ppermute(x, 'ra', shift_pairs(ra, *level, step))]
    pallas_call x4, Pallas kernels: 12.8 us -> 4.33 us  [down(): pl.pallas_call(functools.partial(down_kernel, plan, units), grid=(1,), ou...]
    unnamed x78 -> x37, local copies, waits for them, and re-layouts: 22.9 us -> 16.1 us
    ppermute x20, starting transfers between devices: 25.5 us -> 28.9 us  [send_ra(): return lax.ppermute(x, 'ra', shift_pairs(ra, *level, step))]
    ppermute x16, waiting for transfers between devices: 13.5 us -> 16.2 us  [send_cb(): return lax.ppermute(x, 'cb', shift_pairs(cb, *level, step))]
    convert_element_type x4, other arithmetic: 2.17 us -> 0.16 us  [scatter_sum(): sum((m[step * per:(step + 1) * per].astype(F32) for m in mine)).astype(BF16)]
    convert_element_type x8, other arithmetic: 2 us -> 0.21 us  [sum_cb(): mine = total.astype(BF16)]
  transfers between devices with their start and end apart: 36 -> 36, of which waited for: 21 -> 23; matrix products, arithmetic and copies ran while one was open for 4% -> 1% of each run, Pallas kernels for 20% -> 6%
where the time goes in v2:
time: 136 us
  waiting for transfers between devices  61.8 us (45%)
  starting transfers between devices  42 us (31%)
  local copies, waits for them, and re-layouts  16.1 us (12%)
  Pallas kernels  14 us (10%)
  other arithmetic  1.68 us (1%)
    ppermute x20, waiting for transfers between devices, send_ra(): return lax.ppermute(x, 'ra', shift_pairs(ra, *level, step))  45.6 us
    ppermute x20, starting transfers between devices, send_ra(): return lax.ppermute(x, 'ra', shift_pairs(ra, *level, step))  28.9 us
    ppermute x16, waiting for transfers between devices, send_cb(): return lax.ppermute(x, 'cb', shift_pairs(cb, *level, step))  16.2 us
    unnamed x37, local copies, waits for them, and re-layouts  16.1 us
    ppermute x16, starting transfers between devices, send_cb(): return lax.ppermute(x, 'cb', shift_pairs(cb, *level, step))  13 us
    pallas_call x3, Pallas kernels, project(): pl.pallas_call(functools.partial(project_kernel, plan, layer, units, half...  8.13 us
    pallas_call x4, Pallas kernels, down(): pl.pallas_call(functools.partial(down_kernel, plan, units), grid=(1,), ou...  4.33 us
  transfers between devices with their start and end apart: 36, of which 23 were waited for; matrix products, arithmetic and copies ran while one was open for 1% of the time, Pallas kernels for 6%

profile of v2, /device:TPU:0, one launch (start us, length us, event | category | flops | bytes accessed | tf_op | source)
XLA Modules:
  0.0 136.0 jit_solution(2570556213062649258)
XLA Ops:
  0.1 2.8 %copy-done.2 = f32[2,768,1056]{1,2,0:T(8,128)S(1)} copy-done((f32[2,768,1056]{1,2,0:T(8,128)S(1)}, f32[2,768,1056]{1,2,0:T(8,128)}, u32[]{:S(2)}) %copy-start.2) | copy-done | bytes 6488088
  2.9 2.8 %copy-done.4 = f32[2,768,1056]{1,2,0:T(8,128)S(1)} copy-done((f32[2,768,1056]{1,2,0:T(8,128)S(1)}, f32[2,768,1056]{1,2,0:T(8,128)}, u32[]{:S(2)}) %copy-start.4) | copy-done | bytes 6488088
  7.5 2.9 %project.3 = (bf16[2,536,128]{2,1,0:T(8,128)(2,1)S(1)}, bf16[2,536,128]{2,1,0:T(8,128)(2,1)S(1)}, bf16[2,536,128]{2,1,0:T(8,128)(2,1)S(1)}, bf16[2,536,128]{2,1,0:T(8,128)(2,1)S(1)}) custom-call(s32[2]{0:T(128)S(1)} %pad_add_fusion.1.ids, bf16[2,128,768]{2,1,0:T(8,128)(2,1)S(1)} %copy-done.7, bf16[2,128,768]{2,1,0:T(8,128)(2,1)S(1)} %copy-done.7, ...), custom_call_target="tpu_custom_call" | custom-call | flops 415236096 | bytes 6488064 | tf_op jit(solution)/shard_map/project/pallas_call | solution.py:136
  10.4 3.1 %collective-permute-start.18 = (bf16[2,536,128]{2,1,0:T(8,128)(2,1)S(1)}, bf16[2,536,128]{2,1,0:T(8,128)(2,1)S(1)}, u32[]{:S(2)}, u32[]{:S(2)}) collective-permute-start(bf16[2,536,128]{2,1,0:T(8,128)(2,1)S(1)} %get-tuple-element.30), channel_id=1, source_target_pairs={{0,8},{8,0},{16,24},{24,16},{1,9},{9,1},{17,25},{25,17},{2,10},{10... | collective-permute-start | bytes 823304 | tf_op jit(solution)/shard_map/ppermute | solution.py:232
  13.6 7.3 %collective-permute-done.18.rest_1_ = bf16[2,536,128]{2,1,0:T(8,128)(2,1)S(1)} collective-permute-done((bf16[2,536,128]{2,1,0:T(8,128)(2,1)S(1)}, bf16[2,536,128]{2,1,0:T(8,128)(2,1)S(1)}, u32[]{:S(2)}, u32[]{:S(2)}) %collective-permute-start.18) | collective-permute-done | bytes 274464 | tf_op jit(solution)/shard_map/ppermute | solution.py:232
  20.9 3.1 %collective-permute-start.19 = (bf16[1,536,128]{2,1,0:T(8,128)(2,1)S(1)}, bf16[1,536,128]{2,1,0:T(8,128)(2,1)S(1)}, u32[]{:S(2)}, u32[]{:S(2)}) collective-permute-start(bf16[1,536,128]{2,1,0:T(8,128)(2,1)S(1)} %add_convert_fusion.1), channel_id=1, source_target_pairs={{0,16},{8,24},{16,0},{24,8},{1,17},{9,25},{17,1},{25,9},{2,18},{10... | collective-permute-start | bytes 411656 | tf_op jit(solution)/shard_map/ppermute | solution.py:232
  24.1 4.8 %collective-permute-done.rest_1_ = bf16[2,536,128]{2,1,0:T(8,128)(2,1)S(1)} collective-permute-done((bf16[2,536,128]{2,1,0:T(8,128)(2,1)S(1)}, bf16[2,536,128]{2,1,0:T(8,128)(2,1)S(1)}, u32[]{:S(2)}, u32[]{:S(2)}) %collective-permute-start) | collective-permute-done | bytes 274464 | tf_op jit(solution)/shard_map/ppermute | solution.py:232
  30.7 2.0 %collective-permute-start.20 = (bf16[264,128]{1,0:T(8,128)(2,1)S(1)}, bf16[264,128]{1,0:T(8,128)(2,1)S(1)}, u32[]{:S(2)}, u32[]{:S(2)}) collective-permute-start(bf16[264,128]{1,0:T(8,128)(2,1)S(1)} %activate.6.rest_0_), channel_id=1, source_target_pairs={{0,16},{8,24},{16,0},{24,8},{1,17},{9,25},{17,1},{25,9},{2,18},{10... | collective-permute-start | bytes 202760 | tf_op jit(solution)/shard_map/ppermute | solution.py:232
  32.7 3.6 %collective-permute-start.21 = (bf16[264,128]{1,0:T(8,128)(2,1)S(1)}, bf16[264,128]{1,0:T(8,128)(2,1)S(1)}, u32[]{:S(2)}, u32[]{:S(2)}) collective-permute-start(bf16[264,128]{1,0:T(8,128)(2,1)S(1)} %activate.6.rest_0_), channel_id=1, source_target_pairs={{0,8},{8,0},{16,24},{24,16},{1,9},{9,1},{17,25},{25,17},{2,10},{10... | collective-permute-start | bytes 202760 | tf_op jit(solution)/shard_map/ppermute | solution.py:232
  36.3 3.1 %collective-permute-done.1.rest_2_ = bf16[1,536,128]{2,1,0:T(8,128)(2,1)S(1)} collective-permute-done((bf16[1,536,128]{2,1,0:T(8,128)(2,1)S(1)}, bf16[1,536,128]{2,1,0:T(8,128)(2,1)S(1)}, u32[]{:S(2)}, u32[]{:S(2)}) %collective-permute-start.1) | collective-permute-done | bytes 137248 | tf_op jit(solution)/shard_map/ppermute | solution.py:232
  40.5 2.0 %collective-permute-start.22 = (bf16[264,128]{1,0:T(8,128)(2,1)S(1)}, bf16[264,128]{1,0:T(8,128)(2,1)S(1)}, u32[]{:S(2)}, u32[]{:S(2)}) collective-permute-start(bf16[264,128]{1,0:T(8,128)(2,1)S(1)} %collective-permute-done.20.rest_1_), channel_id=1, source_target_pairs={{0,8},{8,0},{16,24},{24,16},{1,9},{9,1},{17,25},{25,17},{2,10},{10... | collective-permute-start | bytes 202760 | tf_op jit(solution)/shard_map/ppermute | solution.py:232
  42.5 3.0 %collective-permute-done.22.rest_3_ = bf16[264,128]{1,0:T(8,128)(2,1)S(1)} collective-permute-done((bf16[264,128]{1,0:T(8,128)(2,1)S(1)}, bf16[264,128]{1,0:T(8,128)(2,1)S(1)}, u32[]{:S(2)}, u32[]{:S(2)}) %collective-permute-start.22) | collective-permute-done | bytes 67616 | tf_op jit(solution)/shard_map/ppermute | solution.py:232
  45.5 2.8 %copy-done = f32[2,1056,768]{2,1,0:T(8,128)S(1)} copy-done((f32[2,1056,768]{2,1,0:T(8,128)S(1)}, f32[2,1056,768]{2,1,0:T(8,128)}, u32[]{:S(2)}) %copy-start) | copy-done | bytes 6488088
  49.5 1.3 collective-permute-start.3
  51.6 3.0 %collective-permute-done.3.rest_2_ = bf16[264,128]{1,0:T(8,128)(2,1)S(1)} collective-permute-done((bf16[264,128]{1,0:T(8,128)(2,1)S(1)}, bf16[264,128]{1,0:T(8,128)(2,1)S(1)}, u32[]{:S(2)}, u32[]{:S(2)}) %collective-permute-start.3) | collective-permute-done | bytes 67616 | tf_op jit(solution)/shard_map/ppermute | solution.py:232
  55.5 2.8 %copy-done.1 = f32[2,1056,768]{2,1,0:T(8,128)S(1)} copy-done((f32[2,1056,768]{2,1,0:T(8,128)S(1)}, f32[2,1056,768]{2,1,0:T(8,128)}, u32[]{:S(2)}) %copy-start.1) | copy-done | bytes 6488088
  58.4 1.1 down.4
  59.6 1.6 %collective-permute-start.24 = (bf16[64,768]{1,0:T(8,128)(2,1)S(1)}, bf16[64,768]{1,0:T(8,128)(2,1)S(1)}, u32[]{:S(2)}, u32[]{:S(2)}) collective-permute-start(bf16[64,768]{1,0:T(8,128)(2,1)S(1)} %add_convert_fusion.8), channel_id=1, source_target_pairs={{0,2},{1,3},{2,0},{3,1},{4,6},{5,7},{6,4},{7,5},{8,10},{9,11},{10,... | collective-permute-start | bytes 294920 | tf_op jit(solution)/shard_map/ppermute | solution.py:235
  61.2 1.2 collective-permute-start.6
  62.4 2.9 %collective-permute-done.24 = bf16[64,768]{1,0:T(8,128)(2,1)S(1)} collective-permute-done((bf16[64,768]{1,0:T(8,128)(2,1)S(1)}, bf16[64,768]{1,0:T(8,128)(2,1)S(1)}, u32[]{:S(2)}, u32[]{:S(2)}) %collective-permute-start.24) | collective-permute-done | bytes 98336 | tf_op jit(solution)/shard_map/ppermute | solution.py:235
  65.3 1.6 %collective-permute-start.25 = (bf16[64,768]{1,0:T(8,128)(2,1)S(1)}, bf16[64,768]{1,0:T(8,128)(2,1)S(1)}, u32[]{:S(2)}, u32[]{:S(2)}) collective-permute-start(bf16[64,768]{1,0:T(8,128)(2,1)S(1)} %add_convert_fusion.7), channel_id=1, source_target_pairs={{0,4},{1,5},{2,6},{3,7},{4,0},{5,1},{6,2},{7,3},{8,12},{9,13},{10,... | collective-permute-start | bytes 294920 | tf_op jit(solution)/shard_map/ppermute | solution.py:235
  67.0 1.6 %collective-permute-start.7 = (bf16[64,768]{1,0:T(8,128)(2,1)S(1)}, bf16[64,768]{1,0:T(8,128)(2,1)S(1)}, u32[]{:S(2)}, u32[]{:S(2)}) collective-permute-start(bf16[64,768]{1,0:T(8,128)(2,1)S(1)} %add_convert_fusion.12), channel_id=1, source_target_pairs={{0,4},{1,5},{2,6},{3,7},{4,0},{5,1},{6,2},{7,3},{8,12},{9,13},{10,... | collective-permute-start | bytes 294920 | tf_op jit(solution)/shard_map/ppermute | solution.py:235
  68.6 2.2 %collective-permute-done.25 = bf16[64,768]{1,0:T(8,128)(2,1)S(1)} collective-permute-done((bf16[64,768]{1,0:T(8,128)(2,1)S(1)}, bf16[64,768]{1,0:T(8,128)(2,1)S(1)}, u32[]{:S(2)}, u32[]{:S(2)}) %collective-permute-start.25) | collective-permute-done | bytes 98336 | tf_op jit(solution)/shard_map/ppermute | solution.py:235
  70.8 1.3 collective-permute-done.7
  72.3 1.3 collective-permute-done.26.other
  73.6 2.8 %copy-done.5 = f32[2,768,1056]{1,2,0:T(8,128)S(1)} copy-done((f32[2,768,1056]{1,2,0:T(8,128)S(1)}, f32[2,768,1056]{1,2,0:T(8,128)}, u32[]{:S(2)}) %copy-start.5) | copy-done | bytes 6488088
  76.5 2.6 %project.5 = (bf16[2,536,128]{2,1,0:T(8,128)(2,1)S(1)}, bf16[2,536,128]{2,1,0:T(8,128)(2,1)S(1)}) custom-call(s32[2]{0:T(128)S(1)} %pad_add_fusion.ids, bf16[64,768]{1,0:T(8,128)(2,1)S(1)} %get-tuple-element.40.own, bf16[64,768]{1,0:T(8,128)(2,1)S(1)} %collective-permute-done.26.other, f32[2,768]{1,0:T(2,128)S(1)} %copy-done.10, ...), custom_call_target="tpu_custom_call" | custom-call | flops 415236096 | bytes 6488064 | tf_op jit(solution)/shard_map/project/pallas_call | solution.py:136
  79.1 1.3 collective-permute-start.27
  80.4 1.3 collective-permute-done.8.other
  81.7 2.6 %project.4 = (bf16[2,536,128]{2,1,0:T(8,128)(2,1)S(1)}, bf16[2,536,128]{2,1,0:T(8,128)(2,1)S(1)}) custom-call(s32[2]{0:T(128)S(1)} %pad_add_fusion.ids, bf16[64,768]{1,0:T(8,128)(2,1)S(1)} %get-tuple-element.39.own, bf16[64,768]{1,0:T(8,128)(2,1)S(1)} %collective-permute-done.8.other, f32[2,768]{1,0:T(2,128)S(1)} %copy-done.10, ...), custom_call_target="tpu_custom_call" | custom-call | flops 415236096 | bytes 6488064 | tf_op jit(solution)/shard_map/project/pallas_call | solution.py:136
  85.2 3.3 %collective-permute-done.27.rest_1_ = bf16[2,536,128]{2,1,0:T(8,128)(2,1)S(1)} collective-permute-done((bf16[2,536,128]{2,1,0:T(8,128)(2,1)S(1)}, bf16[2,536,128]{2,1,0:T(8,128)(2,1)S(1)}, u32[]{:S(2)}, u32[]{:S(2)}) %collective-permute-start.27) | collective-permute-done | bytes 274464 | tf_op jit(solution)/shard_map/ppermute | solution.py:232
  88.5 1.8 %collective-permute-start.28 = (bf16[1,536,128]{2,1,0:T(8,128)(2,1)S(1)}, bf16[1,536,128]{2,1,0:T(8,128)(2,1)S(1)}, u32[]{:S(2)}, u32[]{:S(2)}) collective-permute-start(bf16[1,536,128]{2,1,0:T(8,128)(2,1)S(1)} %add_convert_fusion), channel_id=1, source_target_pairs={{0,16},{8,24},{16,0},{24,8},{1,17},{9,25},{17,1},{25,9},{2,18},{10... | collective-permute-start | bytes 411656 | tf_op jit(solution)/shard_map/ppermute | solution.py:232
  90.3 6.3 %collective-permute-done.9.rest_1_ = bf16[2,536,128]{2,1,0:T(8,128)(2,1)S(1)} collective-permute-done((bf16[2,536,128]{2,1,0:T(8,128)(2,1)S(1)}, bf16[2,536,128]{2,1,0:T(8,128)(2,1)S(1)}, u32[]{:S(2)}, u32[]{:S(2)}) %collective-permute-start.9) | collective-permute-done | bytes 274464 | tf_op jit(solution)/shard_map/ppermute | solution.py:232
  97.1 3.0 %collective-permute-start.29 = (bf16[264,128]{1,0:T(8,128)(2,1)S(1)}, bf16[264,128]{1,0:T(8,128)(2,1)S(1)}, u32[]{:S(2)}, u32[]{:S(2)}) collective-permute-start(bf16[264,128]{1,0:T(8,128)(2,1)S(1)} %activate.7.rest_0_), channel_id=1, source_target_pairs={{0,16},{8,24},{16,0},{24,8},{1,17},{9,25},{17,1},{25,9},{2,18},{10... | collective-permute-start | bytes 202760 | tf_op jit(solution)/shard_map/ppermute | solution.py:232
  100.1 7.3 %collective-permute-done.29.rest_1_ = bf16[264,128]{1,0:T(8,128)(2,1)S(1)} collective-permute-done((bf16[264,128]{1,0:T(8,128)(2,1)S(1)}, bf16[264,128]{1,0:T(8,128)(2,1)S(1)}, u32[]{:S(2)}, u32[]{:S(2)}) %collective-permute-start.29) | collective-permute-done | bytes 67616 | tf_op jit(solution)/shard_map/ppermute | solution.py:232
  107.8 2.8 %collective-permute-start.11 = (bf16[264,128]{1,0:T(8,128)(2,1)S(1)}, bf16[264,128]{1,0:T(8,128)(2,1)S(1)}, u32[]{:S(2)}, u32[]{:S(2)}) collective-permute-start(bf16[264,128]{1,0:T(8,128)(2,1)S(1)} %activate.5.rest_0_), channel_id=1, source_target_pairs={{0,16},{8,24},{16,0},{24,8},{1,17},{9,25},{17,1},{25,9},{2,18},{10... | collective-permute-start | bytes 202760 | tf_op jit(solution)/shard_map/ppermute | solution.py:232
  110.6 2.0 %collective-permute-done.31.rest_3_ = bf16[264,128]{1,0:T(8,128)(2,1)S(1)} collective-permute-done((bf16[264,128]{1,0:T(8,128)(2,1)S(1)}, bf16[264,128]{1,0:T(8,128)(2,1)S(1)}, u32[]{:S(2)}, u32[]{:S(2)}) %collective-permute-start.31) | collective-permute-done | bytes 67616 | tf_op jit(solution)/shard_map/ppermute | solution.py:232
  112.6 1.1 down.7
  113.9 2.0 %collective-permute-start.13 = (bf16[264,128]{1,0:T(8,128)(2,1)S(1)}, bf16[264,128]{1,0:T(8,128)(2,1)S(1)}, u32[]{:S(2)}, u32[]{:S(2)}) collective-permute-start(bf16[264,128]{1,0:T(8,128)(2,1)S(1)} %collective-permute-done.11.rest_1_), channel_id=1, source_target_pairs={{0,8},{8,0},{16,24},{24,16},{1,9},{9,1},{17,25},{25,17},{2,10},{10... | collective-permute-start | bytes 202760 | tf_op jit(solution)/shard_map/ppermute | solution.py:232
  115.9 3.0 %collective-permute-done.12.rest_2_ = bf16[264,128]{1,0:T(8,128)(2,1)S(1)} collective-permute-done((bf16[264,128]{1,0:T(8,128)(2,1)S(1)}, bf16[264,128]{1,0:T(8,128)(2,1)S(1)}, u32[]{:S(2)}, u32[]{:S(2)}) %collective-permute-start.12) | collective-permute-done | bytes 67616 | tf_op jit(solution)/shard_map/ppermute | solution.py:232
  119.8 1.1 down.5
  121.0 1.6 %collective-permute-start.33 = (bf16[64,768]{1,0:T(8,128)(2,1)S(1)}, bf16[64,768]{1,0:T(8,128)(2,1)S(1)}, u32[]{:S(2)}, u32[]{:S(2)}) collective-permute-start(bf16[64,768]{1,0:T(8,128)(2,1)S(1)} %add_convert_fusion.6), channel_id=1, source_target_pairs={{0,2},{1,3},{2,0},{3,1},{4,6},{5,7},{6,4},{7,5},{8,10},{9,11},{10,... | collective-permute-start | bytes 294920 | tf_op jit(solution)/shard_map/ppermute | solution.py:235
  122.6 1.2 collective-permute-start.15
  123.8 2.9 %collective-permute-done.33 = bf16[64,768]{1,0:T(8,128)(2,1)S(1)} collective-permute-done((bf16[64,768]{1,0:T(8,128)(2,1)S(1)}, bf16[64,768]{1,0:T(8,128)(2,1)S(1)}, u32[]{:S(2)}, u32[]{:S(2)}) %collective-permute-start.33) | collective-permute-done | bytes 98336 | tf_op jit(solution)/shard_map/ppermute | solution.py:235
  126.7 1.8 %collective-permute-start.34 = (bf16[64,768]{1,0:T(8,128)(2,1)S(1)}, bf16[64,768]{1,0:T(8,128)(2,1)S(1)}, u32[]{:S(2)}, u32[]{:S(2)}) collective-permute-start(bf16[64,768]{1,0:T(8,128)(2,1)S(1)} %add_convert_fusion.5), channel_id=1, source_target_pairs={{0,4},{1,5},{2,6},{3,7},{4,0},{5,1},{6,2},{7,3},{8,12},{9,13},{10,... | collective-permute-start | bytes 294920 | tf_op jit(solution)/shard_map/ppermute | solution.py:235
  128.5 1.6 %collective-permute-start.16 = (bf16[64,768]{1,0:T(8,128)(2,1)S(1)}, bf16[64,768]{1,0:T(8,128)(2,1)S(1)}, u32[]{:S(2)}, u32[]{:S(2)}) collective-permute-start(bf16[64,768]{1,0:T(8,128)(2,1)S(1)} %add_convert_fusion.10), channel_id=1, source_target_pairs={{0,4},{1,5},{2,6},{3,7},{4,0},{5,1},{6,2},{7,3},{8,12},{9,13},{10,... | collective-permute-start | bytes 294920 | tf_op jit(solution)/shard_map/ppermute | solution.py:235
  130.1 2.1 %collective-permute-done.34 = bf16[64,768]{1,0:T(8,128)(2,1)S(1)} collective-permute-done((bf16[64,768]{1,0:T(8,128)(2,1)S(1)}, bf16[64,768]{1,0:T(8,128)(2,1)S(1)}, u32[]{:S(2)}, u32[]{:S(2)}) %collective-permute-start.34) | collective-permute-done | bytes 98336 | tf_op jit(solution)/shard_map/ppermute | solution.py:235
  132.2 1.3 collective-permute-done.16
  (96 shorter events, 13.6 us)
Async XLA Ops:
  7.4 22.6 %copy-start.11 = (f32[2,3,1056]{2,0,1:T(2,128)S(1)}, f32[2,3,1056]{2,0,1:T(2,128)}, u32[]{:S(2)}) copy-start(f32[2,3,1056]{2,0,1:T(2,128)} %param.16) | copy-start | bytes 76036
  7.4 22.6 %copy-start.12 = (f32[2,1056]{1,0:T(2,128)S(1)}, f32[2,1056]{1,0:T(2,128)}, u32[]{:S(2)}) copy-start(f32[2,1056]{1,0:T(2,128)} %param.13) | copy-start | bytes 25348
  7.5 22.6 %copy-start.13 = (f32[2,1056]{1,0:T(2,128)S(1)}, f32[2,1056]{1,0:T(2,128)}, u32[]{:S(2)}) copy-start(f32[2,1056]{1,0:T(2,128)} %param.15) | copy-start | bytes 25348
  7.5 22.6 %copy-start.14 = (f32[2,1056]{1,0:T(2,128)S(1)}, f32[2,1056]{1,0:T(2,128)}, u32[]{:S(2)}) copy-start(f32[2,1056]{1,0:T(2,128)} %param.17) | copy-start | bytes 25348
  10.4 10.5 %collective-permute-start.18 = (bf16[2,536,128]{2,1,0:T(8,128)(2,1)S(1)}, bf16[2,536,128]{2,1,0:T(8,128)(2,1)S(1)}, u32[]{:S(2)}, u32[]{:S(2)}) collective-permute-start(bf16[2,536,128]{2,1,0:T(8,128)(2,1)S(1)} %get-tuple-element.30), channel_id=1, source_target_pairs={{0,8},{8,0},{16,24},{24,16},{1,9},{9,1},{17,25},{25,17},{2,10},{10... | collective-permute-start | bytes 823304 | tf_op jit(solution)/shard_map/ppermute | solution.py:232
  13.5 15.4 %collective-permute-start = (bf16[2,536,128]{2,1,0:T(8,128)(2,1)S(1)}, bf16[2,536,128]{2,1,0:T(8,128)(2,1)S(1)}, u32[]{:S(2)}, u32[]{:S(2)}) collective-permute-start(bf16[2,536,128]{2,1,0:T(8,128)(2,1)S(1)} %get-tuple-element.22), channel_id=1, source_target_pairs={{0,8},{8,0},{16,24},{24,16},{1,9},{9,1},{17,25},{25,17},{2,10},{10... | collective-permute-start | bytes 823304 | tf_op jit(solution)/shard_map/ppermute | solution.py:232
  20.9 9.3 %collective-permute-start.19 = (bf16[1,536,128]{2,1,0:T(8,128)(2,1)S(1)}, bf16[1,536,128]{2,1,0:T(8,128)(2,1)S(1)}, u32[]{:S(2)}, u32[]{:S(2)}) collective-permute-start(bf16[1,536,128]{2,1,0:T(8,128)(2,1)S(1)} %add_convert_fusion.1), channel_id=1, source_target_pairs={{0,16},{8,24},{16,0},{24,8},{1,17},{9,25},{17,1},{25,9},{2,18},{10... | collective-permute-start | bytes 411656 | tf_op jit(solution)/shard_map/ppermute | solution.py:232
  28.9 10.5 %collective-permute-start.1 = (bf16[1,536,128]{2,1,0:T(8,128)(2,1)S(1)}, bf16[1,536,128]{2,1,0:T(8,128)(2,1)S(1)}, u32[]{:S(2)}, u32[]{:S(2)}) collective-permute-start(bf16[1,536,128]{2,1,0:T(8,128)(2,1)S(1)} %add_convert_fusion.3), channel_id=1, source_target_pairs={{0,16},{8,24},{16,0},{24,8},{1,17},{9,25},{17,1},{25,9},{2,18},{10... | collective-permute-start | bytes 411656 | tf_op jit(solution)/shard_map/ppermute | solution.py:232
  30.7 9.8 %collective-permute-start.20 = (bf16[264,128]{1,0:T(8,128)(2,1)S(1)}, bf16[264,128]{1,0:T(8,128)(2,1)S(1)}, u32[]{:S(2)}, u32[]{:S(2)}) collective-permute-start(bf16[264,128]{1,0:T(8,128)(2,1)S(1)} %activate.6.rest_0_), channel_id=1, source_target_pairs={{0,16},{8,24},{16,0},{24,8},{1,17},{9,25},{17,1},{25,9},{2,18},{10... | collective-permute-start | bytes 202760 | tf_op jit(solution)/shard_map/ppermute | solution.py:232
  32.7 9.8 %collective-permute-start.21 = (bf16[264,128]{1,0:T(8,128)(2,1)S(1)}, bf16[264,128]{1,0:T(8,128)(2,1)S(1)}, u32[]{:S(2)}, u32[]{:S(2)}) collective-permute-start(bf16[264,128]{1,0:T(8,128)(2,1)S(1)} %activate.6.rest_0_), channel_id=1, source_target_pairs={{0,8},{8,0},{16,24},{24,16},{1,9},{9,1},{17,25},{25,17},{2,10},{10... | collective-permute-start | bytes 202760 | tf_op jit(solution)/shard_map/ppermute | solution.py:232
  39.8 11.0 %collective-permute-start.2 = (bf16[264,128]{1,0:T(8,128)(2,1)S(1)}, bf16[264,128]{1,0:T(8,128)(2,1)S(1)}, u32[]{:S(2)}, u32[]{:S(2)}) collective-permute-start(bf16[264,128]{1,0:T(8,128)(2,1)S(1)} %activate.4.rest_0_), channel_id=1, source_target_pairs={{0,16},{8,24},{16,0},{24,8},{1,17},{9,25},{17,1},{25,9},{2,18},{10... | collective-permute-start | bytes 202760 | tf_op jit(solution)/shard_map/ppermute | solution.py:232
  40.5 5.0 %collective-permute-start.22 = (bf16[264,128]{1,0:T(8,128)(2,1)S(1)}, bf16[264,128]{1,0:T(8,128)(2,1)S(1)}, u32[]{:S(2)}, u32[]{:S(2)}) collective-permute-start(bf16[264,128]{1,0:T(8,128)(2,1)S(1)} %collective-permute-done.20.rest_1_), channel_id=1, source_target_pairs={{0,8},{8,0},{16,24},{24,16},{1,9},{9,1},{17,25},{25,17},{2,10},{10... | collective-permute-start | bytes 202760 | tf_op jit(solution)/shard_map/ppermute | solution.py:232
  48.4 20.2 %copy-start.15 = (f32[2,768]{1,0:T(2,128)S(1)}, f32[2,768]{1,0:T(2,128)}, u32[]{:S(2)}) copy-start(f32[2,768]{1,0:T(2,128)} %param.19) | copy-start | bytes 18436
  48.4 23.8 %copy-start.8 = (bf16[2,128,768]{2,1,0:T(8,128)(2,1)S(1)}, bf16[2,128,768]{2,1,0:T(8,128)(2,1)}, u32[]{:S(2)}) copy-start(bf16[2,128,768]{2,1,0:T(8,128)(2,1)} %other.1) | copy-start | bytes 1179652
  48.4 25.3 %copy-start.10 = (f32[2,768]{1,0:T(2,128)S(1)}, f32[2,768]{1,0:T(2,128)}, u32[]{:S(2)}) copy-start(f32[2,768]{1,0:T(2,128)} %gain.5) | copy-start | bytes 18436
  49.5 10.1 %collective-permute-start.23 = (bf16[64,768]{1,0:T(8,128)(2,1)S(1)}, bf16[64,768]{1,0:T(8,128)(2,1)S(1)}, u32[]{:S(2)}, u32[]{:S(2)}) collective-permute-start(bf16[64,768]{1,0:T(8,128)(2,1)S(1)} %get-tuple-element.32), channel_id=1, source_target_pairs={{0,1},{1,0},{2,3},{3,2},{4,5},{5,4},{6,7},{7,6},{8,9},{9,8},{10,11... | collective-permute-start | bytes 294920 | tf_op jit(solution)/shard_map/ppermute | solution.py:235
  49.5 5.0 %collective-permute-start.3 = (bf16[264,128]{1,0:T(8,128)(2,1)S(1)}, bf16[264,128]{1,0:T(8,128)(2,1)S(1)}, u32[]{:S(2)}, u32[]{:S(2)}) collective-permute-start(bf16[264,128]{1,0:T(8,128)(2,1)S(1)} %activate.4.rest_0_), channel_id=1, source_target_pairs={{0,8},{8,0},{16,24},{24,16},{1,9},{9,1},{17,25},{25,17},{2,10},{10... | collective-permute-start | bytes 202760 | tf_op jit(solution)/shard_map/ppermute | solution.py:232
  50.8 4.7 %collective-permute-start.4 = (bf16[264,128]{1,0:T(8,128)(2,1)S(1)}, bf16[264,128]{1,0:T(8,128)(2,1)S(1)}, u32[]{:S(2)}, u32[]{:S(2)}) collective-permute-start(bf16[264,128]{1,0:T(8,128)(2,1)S(1)} %collective-permute-done.2.rest_1_), channel_id=1, source_target_pairs={{0,8},{8,0},{16,24},{24,16},{1,9},{9,1},{17,25},{25,17},{2,10},{10... | collective-permute-start | bytes 202760 | tf_op jit(solution)/shard_map/ppermute | solution.py:232
  58.4 15.3 %copy-start.3 = (f32[2,768,1056]{1,2,0:T(8,128)S(1)}, f32[2,768,1056]{1,2,0:T(8,128)}, u32[]{:S(2)}) copy-start(f32[2,768,1056]{1,2,0:T(8,128)} %param.12) | copy-start | bytes 19464196
  59.5 1.7 %collective-permute-start.5 = (bf16[64,768]{1,0:T(8,128)(2,1)S(1)}, bf16[64,768]{1,0:T(8,128)(2,1)S(1)}, u32[]{:S(2)}, u32[]{:S(2)}) collective-permute-start(bf16[64,768]{1,0:T(8,128)(2,1)S(1)} %get-tuple-element.24), channel_id=1, source_target_pairs={{0,1},{1,0},{2,3},{3,2},{4,5},{5,4},{6,7},{7,6},{8,9},{9,8},{10,11... | collective-permute-start | bytes 294920 | tf_op jit(solution)/shard_map/ppermute | solution.py:235
  59.6 5.7 %collective-permute-start.24 = (bf16[64,768]{1,0:T(8,128)(2,1)S(1)}, bf16[64,768]{1,0:T(8,128)(2,1)S(1)}, u32[]{:S(2)}, u32[]{:S(2)}) collective-permute-start(bf16[64,768]{1,0:T(8,128)(2,1)S(1)} %add_convert_fusion.8), channel_id=1, source_target_pairs={{0,2},{1,3},{2,0},{3,1},{4,6},{5,7},{6,4},{7,5},{8,10},{9,11},{10,... | collective-permute-start | bytes 294920 | tf_op jit(solution)/shard_map/ppermute | solution.py:235
  61.2 5.8 %collective-permute-start.6 = (bf16[64,768]{1,0:T(8,128)(2,1)S(1)}, bf16[64,768]{1,0:T(8,128)(2,1)S(1)}, u32[]{:S(2)}, u32[]{:S(2)}) collective-permute-start(bf16[64,768]{1,0:T(8,128)(2,1)S(1)} %add_convert_fusion.13), channel_id=1, source_target_pairs={{0,2},{1,3},{2,0},{3,1},{4,6},{5,7},{6,4},{7,5},{8,10},{9,11},{10,... | collective-permute-start | bytes 294920 | tf_op jit(solution)/shard_map/ppermute | solution.py:235
  65.3 5.5 %collective-permute-start.25 = (bf16[64,768]{1,0:T(8,128)(2,1)S(1)}, bf16[64,768]{1,0:T(8,128)(2,1)S(1)}, u32[]{:S(2)}, u32[]{:S(2)}) collective-permute-start(bf16[64,768]{1,0:T(8,128)(2,1)S(1)} %add_convert_fusion.7), channel_id=1, source_target_pairs={{0,4},{1,5},{2,6},{3,7},{4,0},{5,1},{6,2},{7,3},{8,12},{9,13},{10,... | collective-permute-start | bytes 294920 | tf_op jit(solution)/shard_map/ppermute | solution.py:235
  67.0 5.2 %collective-permute-start.7 = (bf16[64,768]{1,0:T(8,128)(2,1)S(1)}, bf16[64,768]{1,0:T(8,128)(2,1)S(1)}, u32[]{:S(2)}, u32[]{:S(2)}) collective-permute-start(bf16[64,768]{1,0:T(8,128)(2,1)S(1)} %add_convert_fusion.12), channel_id=1, source_target_pairs={{0,4},{1,5},{2,6},{3,7},{4,0},{5,1},{6,2},{7,3},{8,12},{9,13},{10,... | collective-permute-start | bytes 294920 | tf_op jit(solution)/shard_map/ppermute | solution.py:235
  72.2 1.4 %collective-permute-start.26 = (bf16[64,768]{1,0:T(8,128)(2,1)S(1)}, bf16[64,768]{1,0:T(8,128)(2,1)S(1)}, u32[]{:S(2)}, u32[]{:S(2)}) collective-permute-start(bf16[64,768]{1,0:T(8,128)(2,1)S(1)} %get-tuple-element.40.own), channel_id=1, source_target_pairs={{0,1},{1,0},{2,3},{3,2},{4,5},{5,4},{6,7},{7,6},{8,9},{9,8},{10,11... | collective-permute-start | bytes 294920 | tf_op jit(solution)/shard_map/ppermute | solution.py:235
  73.6 2.8 %copy-start.5 = (f32[2,768,1056]{1,2,0:T(8,128)S(1)}, f32[2,768,1056]{1,2,0:T(8,128)}, u32[]{:S(2)}) copy-start(f32[2,768,1056]{1,2,0:T(8,128)} %param.14) | copy-start | bytes 19464196
  76.5 5.2 %copy-start.6 = (f32[2,768,1056]{1,2,0:T(8,128)S(1)}, f32[2,768,1056]{1,2,0:T(8,128)}, u32[]{:S(2)}) copy-start(f32[2,768,1056]{1,2,0:T(8,128)} %param.14) | copy-start | bytes 19464196
  79.1 9.4 %collective-permute-start.27 = (bf16[2,536,128]{2,1,0:T(8,128)(2,1)S(1)}, bf16[2,536,128]{2,1,0:T(8,128)(2,1)S(1)}, u32[]{:S(2)}, u32[]{:S(2)}) collective-permute-start(bf16[2,536,128]{2,1,0:T(8,128)(2,1)S(1)} %get-tuple-element.34), channel_id=1, source_target_pairs={{0,8},{8,0},{16,24},{24,16},{1,9},{9,1},{17,25},{25,17},{2,10},{10... | collective-permute-start | bytes 823304 | tf_op jit(solution)/shard_map/ppermute | solution.py:232
  80.4 32.2 %slice-start = ((s8[6488064]{0:T(1024)(128)(4,1)}), s8[4194304]{0:T(1024)(128)(4,1)S(1)}, s32[]{:S(2)}) async-start(s8[6488064]{0:T(1024)(128)(4,1)} %bitcast.24), calls=%async_computation | async-start | bytes 8388608
  80.4 32.2 %slice-start.1 = ((s8[6488064]{0:T(1024)(128)(4,1)}), s8[2293760]{0:T(1024)(128)(4,1)S(1)}, s32[]{:S(2)}) async-start(s8[6488064]{0:T(1024)(128)(4,1)} %bitcast.24), calls=%async_computation.1 | async-start | bytes 4587520
  80.4 1.3 collective-permute-start.8
  84.3 12.3 %collective-permute-start.9 = (bf16[2,536,128]{2,1,0:T(8,128)(2,1)S(1)}, bf16[2,536,128]{2,1,0:T(8,128)(2,1)S(1)}, u32[]{:S(2)}, u32[]{:S(2)}) collective-permute-start(bf16[2,536,128]{2,1,0:T(8,128)(2,1)S(1)} %get-tuple-element.26), channel_id=1, source_target_pairs={{0,8},{8,0},{16,24},{24,16},{1,9},{9,1},{17,25},{25,17},{2,10},{10... | collective-permute-start | bytes 823304 | tf_op jit(solution)/shard_map/ppermute | solution.py:232
  88.5 8.2 %collective-permute-start.28 = (bf16[1,536,128]{2,1,0:T(8,128)(2,1)S(1)}, bf16[1,536,128]{2,1,0:T(8,128)(2,1)S(1)}, u32[]{:S(2)}, u32[]{:S(2)}) collective-permute-start(bf16[1,536,128]{2,1,0:T(8,128)(2,1)S(1)} %add_convert_fusion), channel_id=1, source_target_pairs={{0,16},{8,24},{16,0},{24,8},{1,17},{9,25},{17,1},{25,9},{2,18},{10... | collective-permute-start | bytes 411656 | tf_op jit(solution)/shard_map/ppermute | solution.py:232
  96.6 10.8 %collective-permute-start.10 = (bf16[1,536,128]{2,1,0:T(8,128)(2,1)S(1)}, bf16[1,536,128]{2,1,0:T(8,128)(2,1)S(1)}, u32[]{:S(2)}, u32[]{:S(2)}) collective-permute-start(bf16[1,536,128]{2,1,0:T(8,128)(2,1)S(1)} %add_convert_fusion.2), channel_id=1, source_target_pairs={{0,16},{8,24},{16,0},{24,8},{1,17},{9,25},{17,1},{25,9},{2,18},{10... | collective-permute-start | bytes 411656 | tf_op jit(solution)/shard_map/ppermute | solution.py:232
  97.1 10.3 %collective-permute-start.29 = (bf16[264,128]{1,0:T(8,128)(2,1)S(1)}, bf16[264,128]{1,0:T(8,128)(2,1)S(1)}, u32[]{:S(2)}, u32[]{:S(2)}) collective-permute-start(bf16[264,128]{1,0:T(8,128)(2,1)S(1)} %activate.7.rest_0_), channel_id=1, source_target_pairs={{0,16},{8,24},{16,0},{24,8},{1,17},{9,25},{17,1},{25,9},{2,18},{10... | collective-permute-start | bytes 202760 | tf_op jit(solution)/shard_map/ppermute | solution.py:232
  100.1 10.5 %collective-permute-start.30 = (bf16[264,128]{1,0:T(8,128)(2,1)S(1)}, bf16[264,128]{1,0:T(8,128)(2,1)S(1)}, u32[]{:S(2)}, u32[]{:S(2)}) collective-permute-start(bf16[264,128]{1,0:T(8,128)(2,1)S(1)} %activate.7.rest_0_), channel_id=1, source_target_pairs={{0,8},{8,0},{16,24},{24,16},{1,9},{9,1},{17,25},{25,17},{2,10},{10... | collective-permute-start | bytes 202760 | tf_op jit(solution)/shard_map/ppermute | solution.py:232
  107.4 5.2 %collective-permute-start.31 = (bf16[264,128]{1,0:T(8,128)(2,1)S(1)}, bf16[264,128]{1,0:T(8,128)(2,1)S(1)}, u32[]{:S(2)}, u32[]{:S(2)}) collective-permute-start(bf16[264,128]{1,0:T(8,128)(2,1)S(1)} %collective-permute-done.29.rest_1_), channel_id=1, source_target_pairs={{0,8},{8,0},{16,24},{24,16},{1,9},{9,1},{17,25},{25,17},{2,10},{10... | collective-permute-start | bytes 202760 | tf_op jit(solution)/shard_map/ppermute | solution.py:232
  107.8 6.1 %collective-permute-start.11 = (bf16[264,128]{1,0:T(8,128)(2,1)S(1)}, bf16[264,128]{1,0:T(8,128)(2,1)S(1)}, u32[]{:S(2)}, u32[]{:S(2)}) collective-permute-start(bf16[264,128]{1,0:T(8,128)(2,1)S(1)} %activate.5.rest_0_), channel_id=1, source_target_pairs={{0,16},{8,24},{16,0},{24,8},{1,17},{9,25},{17,1},{25,9},{2,18},{10... | collective-permute-start | bytes 202760 | tf_op jit(solution)/shard_map/ppermute | solution.py:232
  113.7 7.2 %collective-permute-start.32 = (bf16[64,768]{1,0:T(8,128)(2,1)S(1)}, bf16[64,768]{1,0:T(8,128)(2,1)S(1)}, u32[]{:S(2)}, u32[]{:S(2)}) collective-permute-start(bf16[64,768]{1,0:T(8,128)(2,1)S(1)} %get-tuple-element.36), channel_id=1, source_target_pairs={{0,1},{1,0},{2,3},{3,2},{4,5},{5,4},{6,7},{7,6},{8,9},{9,8},{10,11... | collective-permute-start | bytes 294920 | tf_op jit(solution)/shard_map/ppermute | solution.py:235
  113.8 5.1 %collective-permute-start.12 = (bf16[264,128]{1,0:T(8,128)(2,1)S(1)}, bf16[264,128]{1,0:T(8,128)(2,1)S(1)}, u32[]{:S(2)}, u32[]{:S(2)}) collective-permute-start(bf16[264,128]{1,0:T(8,128)(2,1)S(1)} %activate.5.rest_0_), channel_id=1, source_target_pairs={{0,8},{8,0},{16,24},{24,16},{1,9},{9,1},{17,25},{25,17},{2,10},{10... | collective-permute-start | bytes 202760 | tf_op jit(solution)/shard_map/ppermute | solution.py:232
  113.9 5.9 %collective-permute-start.13 = (bf16[264,128]{1,0:T(8,128)(2,1)S(1)}, bf16[264,128]{1,0:T(8,128)(2,1)S(1)}, u32[]{:S(2)}, u32[]{:S(2)}) collective-permute-start(bf16[264,128]{1,0:T(8,128)(2,1)S(1)} %collective-permute-done.11.rest_1_), channel_id=1, source_target_pairs={{0,8},{8,0},{16,24},{24,16},{1,9},{9,1},{17,25},{25,17},{2,10},{10... | collective-permute-start | bytes 202760 | tf_op jit(solution)/shard_map/ppermute | solution.py:232
  120.9 1.7 %collective-permute-start.14 = (bf16[64,768]{1,0:T(8,128)(2,1)S(1)}, bf16[64,768]{1,0:T(8,128)(2,1)S(1)}, u32[]{:S(2)}, u32[]{:S(2)}) collective-permute-start(bf16[64,768]{1,0:T(8,128)(2,1)S(1)} %get-tuple-element.28), channel_id=1, source_target_pairs={{0,1},{1,0},{2,3},{3,2},{4,5},{5,4},{6,7},{7,6},{8,9},{9,8},{10,11... | collective-permute-start | bytes 294920 | tf_op jit(solution)/shard_map/ppermute | solution.py:235
  121.0 5.7 %collective-permute-start.33 = (bf16[64,768]{1,0:T(8,128)(2,1)S(1)}, bf16[64,768]{1,0:T(8,128)(2,1)S(1)}, u32[]{:S(2)}, u32[]{:S(2)}) collective-permute-start(bf16[64,768]{1,0:T(8,128)(2,1)S(1)} %add_convert_fusion.6), channel_id=1, source_target_pairs={{0,2},{1,3},{2,0},{3,1},{4,6},{5,7},{6,4},{7,5},{8,10},{9,11},{10,... | collective-permute-start | bytes 294920 | tf_op jit(solution)/shard_map/ppermute | solution.py:235
  122.6 5.9 %collective-permute-start.15 = (bf16[64,768]{1,0:T(8,128)(2,1)S(1)}, bf16[64,768]{1,0:T(8,128)(2,1)S(1)}, u32[]{:S(2)}, u32[]{:S(2)}) collective-permute-start(bf16[64,768]{1,0:T(8,128)(2,1)S(1)} %add_convert_fusion.11), channel_id=1, source_target_pairs={{0,2},{1,3},{2,0},{3,1},{4,6},{5,7},{6,4},{7,5},{8,10},{9,11},{10,... | collective-permute-start | bytes 294920 | tf_op jit(solution)/shard_map/ppermute | solution.py:235
  126.7 5.5 %collective-permute-start.34 = (bf16[64,768]{1,0:T(8,128)(2,1)S(1)}, bf16[64,768]{1,0:T(8,128)(2,1)S(1)}, u32[]{:S(2)}, u32[]{:S(2)}) collective-permute-start(bf16[64,768]{1,0:T(8,128)(2,1)S(1)} %add_convert_fusion.5), channel_id=1, source_target_pairs={{0,4},{1,5},{2,6},{3,7},{4,0},{5,1},{6,2},{7,3},{8,12},{9,13},{10,... | collective-permute-start | bytes 294920 | tf_op jit(solution)/shard_map/ppermute | solution.py:235
  128.5 5.0 %collective-permute-start.16 = (bf16[64,768]{1,0:T(8,128)(2,1)S(1)}, bf16[64,768]{1,0:T(8,128)(2,1)S(1)}, u32[]{:S(2)}, u32[]{:S(2)}) collective-permute-start(bf16[64,768]{1,0:T(8,128)(2,1)S(1)} %add_convert_fusion.10), channel_id=1, source_target_pairs={{0,4},{1,5},{2,6},{3,7},{4,0},{5,1},{6,2},{7,3},{8,12},{9,13},{10,... | collective-permute-start | bytes 294920 | tf_op jit(solution)/shard_map/ppermute | solution.py:235
  133.6 1.4 %collective-permute-start.17 = (bf16[64,768]{1,0:T(8,128)(2,1)S(1)}, bf16[64,768]{1,0:T(8,128)(2,1)S(1)}, u32[]{:S(2)}, u32[]{:S(2)}) collective-permute-start(bf16[64,768]{1,0:T(8,128)(2,1)S(1)} %get-tuple-element.45), channel_id=1, source_target_pairs={{0,1},{1,0},{2,3},{3,2},{4,5},{5,4},{6,7},{7,6},{8,9},{9,8},{10,11... | collective-permute-start | bytes 294920 | tf_op jit(solution)/shard_map/ppermute | solution.py:235
  133.7 1.4 %collective-permute-start.35 = (bf16[64,768]{1,0:T(8,128)(2,1)S(1)}, bf16[64,768]{1,0:T(8,128)(2,1)S(1)}, u32[]{:S(2)}, u32[]{:S(2)}) collective-permute-start(bf16[64,768]{1,0:T(8,128)(2,1)S(1)} %get-tuple-element.46), channel_id=1, source_target_pairs={{0,1},{1,0},{2,3},{3,2},{4,5},{5,4},{6,7},{7,6},{8,9},{9,8},{10,11... | collective-permute-start | bytes 294920 | tf_op jit(solution)/shard_map/ppermute | solution.py:235
  (6 other events, 13.1 us)
